TPU v7x, 32 devices: a whole 2x2x4 slice. The times are simulated.
32 devices in a mesh: grp: 2 (over y), ep: 8 (over z, core), tp: 2 (over x).
Axes of the slice: x: 2, y: 2, z: 4, core: 2. Of those that a mesh axis runs over, the one named last changes fastest.
Arguments:
- tokens: bfloat16 [2048, 4096], P(('grp', 'ep'), 'tp'), parts along dimension 0, may hold values from -6 to 6
- routes: int32 [2048, 4], P(('grp', 'ep')), parts along dimension 0, may hold values from 0 to 7, all different within a row; in each aligned block of 128 rows (0 to 127, 128 to 255, ...) at most 128 rows name the same one
- route_weights: float32 [2048, 4], P(('grp', 'ep')), parts along dimension 0, may hold values from 0.1 to 1
- norm_gain: float32 [4096], replicated, may hold values from 0.1 to 1.9
- expert_gate: bfloat16 [8, 4096, 1024], P('ep', 'tp'), may hold values from -0.09375 to 0.09375
- expert_up: bfloat16 [8, 4096, 1024], P('ep', 'tp'), may hold values from -0.09375 to 0.09375
- expert_down: bfloat16 [8, 1024, 4096], P('ep', None, 'tp')
- shared_gate: bfloat16 [4096, 1024], P('tp'), may hold values from -0.09375 to 0.09375
- shared_up: bfloat16 [4096, 1024], P('tp'), may hold values from -0.09375 to 0.09375
- shared_down: bfloat16 [1024, 4096], P(None, 'tp')
- out_gain: float32 [4096], P('tp'), may hold values from 0.1 to 1.9
Outputs:
- layer_out: bfloat16 [2048, 4096], P(('grp', 'ep'), 'tp'), parts along dimension 0
There are 2 independent parts, one for each index of `grp`. A program takes and returns all parts, laid end to end along the dimension named above; an argument that names none is the same for every part. Nothing has to cross between parts.
Inputs may be any that keep to these rules, and one draw needn't show every extreme that they name: `routes`: each row names 4 different experts; among the rows of one index of ep no expert is named more than 128 times, and in some such block some expert is named exactly 128 times.
All inputs are finite; a program needn't handle non-finite values.
Results may differ from a plain program's by a relative error of at most 0.023.
Values may be sent and summed in bfloat16 or wider, within the bound.
A program may use at most 64 MiB of HBM per device.

v0:
```python
import functools

import jax
import jax.numpy as jnp
from jax import lax
from jax.experimental import pallas as pl
from jax.experimental.pallas import tpu as pltpu
from jax.sharding import PartitionSpec as P

epsilon = 1e-06
MESH = pl.DeviceIdType.MESH
TABLE = 128


def plan(chips):
    ring = [mask for mask in range(2, chips)]
    first = [(0, 0), (0, 1), (1, 0)]
    steps = first + [(mask, 0) for mask in ring] + [(mask, 1) for mask in ring] + [(1, 1), None]
    relays = [[steps.index((distance, 0)), steps.index((max(distance, 2), 1))] for distance in range(1, chips)]
    relays[0][1] -= 1
    return steps, relays


def pick(index, table):
    value = jnp.int32(table[0])
    for position in range(1, len(table)):
        if table[position] != table[0]:
            value = jnp.where(index == position, jnp.int32(table[position]), value)
    return value


def exclusive_or(a, b, size):
    total, unit = jnp.int32(0), 1
    while unit < size:
        total = total + unit * lax.rem(lax.div(a, unit) + lax.div(b, unit), 2)
        unit *= 2
    return total


def fused_kernel(
    chips,
    tokens_hbm,
    routes_hbm,
    weights_hbm,
    norm_gain_hbm,
    gate_hbm,
    up_hbm,
    down_hbm,
    shared_gate_hbm,
    shared_up_hbm,
    shared_down_hbm,
    out_gain_hbm,
    out_ref,
    tokens_ref,
    routes_ref,
    weights_ref,
    norm_gain_ref,
    out_gain_ref,
    gate,
    up,
    down,
    held,
    part_out,
    part_in,
    part_own,
    hidden,
    product,
    waiting,
    pair_out,
    pair_in,
    far_out,
    far_in,
    mixture,
    square_out,
    square_in,
    load_sem,
    square_send,
    square_recv,
    gather_send,
    gather_recv,
    pair_gather_recv,
    part_send,
    part_recv,
    hidden_send,
    hidden_recv,
    pair_send,
    pair_recv,
    far_send,
    far_recv,
):
    rows, width = tokens_ref.shape
    experts = 2 * chips
    units = gate.shape[2]
    half = units // 2
    steps, relays = plan(chips)
    count = len(steps)
    masks = [0 if s is None else s[0] for s in steps]
    lanes = [0 if s is None else s[1] for s in steps]
    shared_at = steps.index(None)

    ep = lax.axis_index("ep")
    tp = lax.axis_index("tp")
    chip, core = lax.div(ep, 2), lax.rem(ep, 2)
    other_core = 1 - core
    partner = {"ep": chip * 2 + other_core}
    across = {"tp": 1 - tp}

    loads = [
        pltpu.make_async_copy(source, target, load_sem.at[i])
        for i, (source, target) in enumerate(
            [
                (gate_hbm.at[0], gate.at[0]),
                (up_hbm.at[0], up.at[0]),
                (shared_gate_hbm, gate.at[1]),
                (shared_up_hbm, up.at[1]),
                (down_hbm.at[0], down.at[0]),
                (shared_down_hbm, down.at[1]),
                (tokens_hbm, tokens_ref),
                (routes_hbm, routes_ref),
                (weights_hbm, weights_ref),
                (norm_gain_hbm, norm_gain_ref),
                (out_gain_hbm, out_gain_ref),
            ]
        )
    ]
    for load in loads[6:] + loads[:2]:
        load.start()

    barrier = pltpu.get_barrier_semaphore()
    for shift in range(1, chips):
        pl.semaphore_signal(
            barrier,
            inc=1,
            device_id={"ep": lax.rem(chip + shift, chips) * 2 + core},
            device_id_type=MESH,
        )
    pl.semaphore_signal(barrier, inc=1, device_id=partner, device_id_type=MESH)
    pl.semaphore_signal(barrier, inc=1, device_id=across, device_id_type=MESH)

    def remote(source, target, send, recv, device):
        return pltpu.make_async_remote_copy(
            src_ref=source,
            dst_ref=target,
            send_sem=send,
            recv_sem=recv,
            device_id=device,
            device_id_type=MESH,
        )

    def square_copy(which):
        return remote(
            square_out.at[which],
            square_in.at[which],
            square_send.at[which],
            square_recv.at[which],
            across,
        )

    def gather_copy(origin, way):
        slot = held.at[origin * 2 + core]
        device = ({"ep": (chip - 1) * 2 + core}, {"ep": (chip + 1) * 2 + core}, partner)[way]
        recv = (pair_gather_recv if way == 2 else gather_recv).at[origin]
        return remote(slot, slot, gather_send.at[origin, way], recv, device)

    def pair_gather_arrival(origin):
        slot = held.at[origin * 2 + other_core]
        return remote(slot, slot, gather_send.at[origin, 2], pair_gather_recv.at[origin], partner)

    def part_copy(k, which):
        return remote(
            part_out.at[k, which],
            part_in.at[k, which],
            part_send.at[k, which],
            part_recv.at[k, which],
            across,
        )

    def hidden_copy(k, side):
        return remote(
            hidden.at[k, side], hidden.at[k, side], hidden_send.at[k], hidden_recv.at[k], across
        )

    def pair_copy(origin):
        return remote(
            pair_out.at[origin],
            pair_in.at[origin],
            pair_send.at[origin],
            pair_recv.at[origin],
            partner,
        )

    beside, opposite, beyond = (exclusive_or(chip, mask, chips) for mask in (1, 2, 3))

    def far_copy(mask, origin):
        slot = jnp.where(mask == 2, beyond, chip)
        return remote(
            far_out.at[origin],
            far_in.at[slot],
            far_send.at[origin],
            far_recv.at[slot],
            {"ep": jnp.where(mask == 3, beyond, beside) * 2 + core},
        )

    def far_arrival(slot):
        return remote(
            far_out.at[slot],
            far_in.at[slot],
            far_send.at[slot],
            far_recv.at[slot],
            {"ep": beside * 2 + core},
        )

    def pack(column):
        return jnp.transpose(jnp.broadcast_to(column, (rows, 128)))[:8]

    def unpack(row):
        return jnp.transpose(jnp.broadcast_to(row[:1], (128, rows)))[:, :1]

    for load in loads[6:]:
        load.wait()
    token_float = tokens_ref[...].astype(jnp.float32)
    own_square = jnp.sum(token_float * token_float, axis=-1, keepdims=True)
    square_out[0] = pack(own_square)
    pl.semaphore_wait(barrier, chips + 1)
    square_copy(0).start()
    lane_ids = lax.broadcasted_iota(jnp.int32, (rows, TABLE), 1)
    expert_ids = lax.broadcasted_iota(jnp.int32, (TABLE, rows), 0)
    table = jnp.zeros((TABLE, rows), jnp.float32)
    for choice in range(routes_ref.shape[0]):
        named = routes_ref[choice : choice + 1, :]
        match = (expert_ids == named) | (expert_ids == named + experts)
        table = table + jnp.where(match, weights_ref[choice : choice + 1, :], 0.0)
    table = jnp.transpose(table)
    coarse = table.astype(jnp.bfloat16).astype(jnp.float32)
    held[ep, :, width:] = jnp.where(lane_ids < experts, table, table - coarse).astype(jnp.bfloat16)
    mixture[...] = jnp.zeros_like(mixture)
    square_copy(0).wait_recv()
    square = own_square + unpack(square_in[0])
    gain = norm_gain_ref[:, pl.ds(pl.multiple_of(tp * width, width), width)]
    held[ep, :, :width] = (
        tokens_ref[...].astype(jnp.float32) * lax.rsqrt(square / (2 * width) + epsilon) * gain
    ).astype(jnp.bfloat16)

    def send_outward():
        @pl.when(chip > 0)
        def _():
            gather_copy(chip, 0).start()

        @pl.when(chip < chips - 1)
        def _():
            gather_copy(chip, 1).start()

    gather_copy(chip, 2).start()
    pl.when(core == 0)(send_outward)

    def locate(k):
        origin = exclusive_or(chip, pick(k, masks), chips)
        lane = pick(k, lanes)
        return origin, lane

    def first_stage(k):
        origin, lane = locate(k)
        is_shared = k == shared_at

        @pl.when(k == 0)
        def _():
            loads[0].wait()
            loads[1].wait()
            for load in loads[2:6]:
                load.start()

        @pl.when(is_shared)
        def _():
            loads[2].wait()
            loads[3].wait()

        for index, positions in enumerate(relays):
            distance = index + 1
            position = jnp.where(core == 0, positions[0], positions[1])

            @pl.when((k == position) & (chip >= distance))
            def _(distance=distance):
                gather_copy(chip - distance, 0).wait_recv()
                gather_copy(chip - distance, 2).start()

                @pl.when(chip < chips - 1)
                def _():
                    gather_copy(chip - distance, 1).start()

            @pl.when((k == position) & (chip + distance < chips))
            def _(distance=distance):
                gather_copy(chip + distance, 1).wait_recv()
                gather_copy(chip + distance, 2).start()

                @pl.when(chip > 0)
                def _():
                    gather_copy(chip + distance, 0).start()

        @pl.when((lane != core) & (k != shared_at))
        def _():
            pair_gather_arrival(origin).wait_recv()

        block = jnp.where(is_shared, ep, origin * 2 + lane)
        kind = jnp.where(is_shared, 1, 0)
        source = held[block, :, :width]
        away = pl.ds(pl.multiple_of((1 - tp) * half, half), half)
        near = pl.ds(pl.multiple_of(tp * half, half), half)
        for which, matrix in enumerate((gate, up)):
            part_out[k, which] = jnp.dot(
                source, matrix[kind, :, away], preferred_element_type=jnp.float32
            ).astype(jnp.bfloat16)
            part_copy(k, which).start()
        for which, matrix in enumerate((gate, up)):
            part_own[k, which] = jnp.dot(
                source, matrix[kind, :, near], preferred_element_type=jnp.float32
            ).astype(jnp.bfloat16)

    def second_stage(k):
        part_copy(k, 0).wait_recv()
        part_copy(k, 1).wait_recv()
        gate_sum = part_own[k, 0].astype(jnp.float32) + part_in[k, 0].astype(jnp.float32)
        up_sum = part_own[k, 1].astype(jnp.float32) + part_in[k, 1].astype(jnp.float32)
        hidden[k, tp] = (jax.nn.silu(gate_sum) * up_sum).astype(jnp.bfloat16)
        hidden_copy(k, tp).start()

    def third_stage(k):
        origin, lane = locate(k)
        is_shared = k == shared_at

        @pl.when(k == 0)
        def _():
            loads[4].wait()
            loads[5].wait()

        hidden_copy(k, 1 - tp).wait_recv()
        block = jnp.where(is_shared, ep, origin * 2 + lane)
        kind = jnp.where(is_shared, 1, 0)
        chosen = (lane_ids == ep) | (lane_ids == ep + experts)
        scale = jnp.sum(
            jnp.where(chosen, held[block, :, width:].astype(jnp.float32), 0.0),
            axis=-1,
            keepdims=True,
        )
        tile = width // 4

        def tile_step(i, carry):
            columns = pl.ds(pl.multiple_of(i * tile, tile), tile)
            product[:, columns] = jnp.dot(
                hidden[k, 0], down[kind, :half, columns], preferred_element_type=jnp.float32
            ) + jnp.dot(
                hidden[k, 1], down[kind, half:, columns], preferred_element_type=jnp.float32
            )
            return carry

        lax.fori_loop(0, 4, tile_step, 0)

        def weighted():
            return product[...].astype(jnp.bfloat16).astype(jnp.float32) * scale

        @pl.when(is_shared)
        def _():
            mixture[...] += product[...]

        @pl.when((k != shared_at) & (lane != core))
        def _():
            pair_out[origin] = weighted().astype(jnp.bfloat16)
            pair_copy(origin).start()

        @pl.when((k != shared_at) & (lane == core))
        def _():
            waiting[...] = weighted()

    def fourth_stage(k):
        origin, lane = locate(k)

        @pl.when((k != shared_at) & (lane == core))
        def _():
            pair_copy(origin).wait_recv()

            @pl.when(origin == chip)
            def _():
                mixture[...] += waiting[...] + pair_in[origin].astype(jnp.float32)

            mask = pick(k, masks)

            @pl.when(mask == 3)
            def _():
                far_arrival(opposite).wait_recv()
                waiting[...] += far_in[opposite].astype(jnp.float32)

            @pl.when(origin != chip)
            def _():
                far_out[origin] = (waiting[...] + pair_in[origin].astype(jnp.float32)).astype(
                    jnp.bfloat16
                )
                far_copy(mask, origin).start()

    def body(i, carry):
        @pl.when(i < count)
        def _():
            first_stage(i)

        @pl.when(i >= 3)
        def _():
            fourth_stage(i - 3)

        @pl.when((i >= 1) & (i < count + 1))
        def _():
            second_stage(i - 1)

        @pl.when((i == 2) & (core == 1))
        def _():
            send_outward()

        @pl.when((i >= 2) & (i < count + 2))
        def _():
            third_stage(i - 2)

        return carry

    lax.fori_loop(0, count + 3, body, 0)

    far_arrival(beside).wait_recv()
    far_arrival(beyond).wait_recv()
    mixture[...] += far_in[beside].astype(jnp.float32) + far_in[beyond].astype(jnp.float32)

    mixed = mixture[...]
    own_total = jnp.sum(mixed * mixed, axis=-1, keepdims=True)
    square_out[1] = pack(own_total)
    square_copy(1).start()
    square_copy(1).wait_recv()
    total = own_total + unpack(square_in[1])
    out_ref[...] = (
        mixture[...] * lax.rsqrt(total / (2 * width) + epsilon) * out_gain_ref[...]
    ).astype(jnp.bfloat16)

    square_copy(0).wait_send()
    square_copy(1).wait_send()
    for origin in range(chips):
        gather_copy(origin, 2).wait_send()
        pair_copy(origin).wait_send()

        @pl.when((chip >= origin) & (chip < chips - 1))
        def _(origin=origin):
            gather_copy(origin, 1).wait_send()

        @pl.when((chip <= origin) & (chip > 0))
        def _(origin=origin):
            gather_copy(origin, 0).wait_send()

        @pl.when(chip != origin)
        def _(origin=origin):
            far_arrival(origin).wait_send()

    def drain(k, carry):
        part_copy(k, 0).wait_send()
        part_copy(k, 1).wait_send()
        hidden_copy(k, tp).wait_send()
        return carry

    lax.fori_loop(0, count, drain, 0)


def fused(
    chips,
    tokens,
    routes,
    route_weights,
    norm_gain,
    expert_gate,
    expert_up,
    expert_down,
    shared_gate,
    shared_up,
    shared_down,
    out_gain,
):
    rows, width = tokens.shape
    units = shared_gate.shape[1]
    half = units // 2
    count = 2 * chips + 1
    choices = routes.shape[1]
    vmem = pl.BlockSpec(memory_space=pltpu.VMEM)
    hbm = pl.BlockSpec(memory_space=pl.ANY)
    bf16, f32 = jnp.bfloat16, jnp.float32
    dma = pltpu.SemaphoreType.DMA
    return pl.pallas_call(
        functools.partial(fused_kernel, chips),
        out_shape=jax.ShapeDtypeStruct((rows, width), bf16),
        in_specs=[hbm] * 11,
        out_specs=vmem,
        scratch_shapes=[
            pltpu.VMEM((rows, width), bf16),
            pltpu.VMEM((choices, rows), jnp.int32),
            pltpu.VMEM((choices, rows), f32),
            pltpu.VMEM((1, norm_gain.shape[0]), f32),
            pltpu.VMEM((1, width), f32),
            pltpu.VMEM((2, width, units), bf16),
            pltpu.VMEM((2, width, units), bf16),
            pltpu.VMEM((2, units, width), bf16),
            pltpu.VMEM((2 * chips, rows, width + TABLE), bf16),
            pltpu.VMEM((count, 2, rows, half), bf16),
            pltpu.VMEM((count, 2, rows, half), bf16),
            pltpu.VMEM((count, 2, rows, half), bf16),
            pltpu.VMEM((count, 2, rows, half), bf16),
            pltpu.VMEM((rows, width), f32),
            pltpu.VMEM((rows, width), f32),
            pltpu.VMEM((chips, rows, width), bf16),
            pltpu.VMEM((chips, rows, width), bf16),
            pltpu.VMEM((chips, rows, width), bf16),
            pltpu.VMEM((chips, rows, width), bf16),
            pltpu.VMEM((rows, width), f32),
            pltpu.VMEM((2, 8, rows), f32),
            pltpu.VMEM((2, 8, rows), f32),
            dma((11,)),
            dma((2,)),
            dma((2,)),
            dma((chips, 3)),
            dma((chips,)),
            dma((chips,)),
            dma((count, 2)),
            dma((count, 2)),
            dma((count,)),
            dma((count,)),
            dma((chips,)),
            dma((chips,)),
            dma((chips,)),
            dma((chips,)),
        ],
        compiler_params=pltpu.CompilerParams(
            collective_id=0, has_side_effects=True, vmem_limit_bytes=60 * 1024 * 1024
        ),
    )(
        tokens,
        routes.T,
        route_weights.T,
        norm_gain.reshape(1, -1),
        expert_gate,
        expert_up,
        expert_down,
        shared_gate,
        shared_up,
        shared_down,
        out_gain.reshape(1, -1),
    )


def local_product(source, matrix):
    return jnp.dot(source, matrix, preferred_element_type=jnp.float32)


def per_device(
    tokens,
    routes,
    route_weights,
    norm_gain,
    expert_gate,
    expert_up,
    expert_down,
    shared_gate,
    shared_up,
    shared_down,
    out_gain,
):
    block_width = tokens.shape[1]
    full_width = block_width * lax.axis_size("tp")
    width_index = lax.axis_index("tp")
    full_rows = lax.all_gather(tokens, "tp", axis=1, tiled=True)
    full_float = full_rows.astype(jnp.float32)
    normed_full = (
        full_float
        * lax.rsqrt(jnp.mean(full_float * full_float, axis=-1, keepdims=True) + epsilon)
        * norm_gain
    ).astype(jnp.bfloat16)
    normed_block = lax.dynamic_slice_in_dim(normed_full, width_index * block_width, block_width, 1)
    gate_matrix = expert_gate[0]
    up_matrix = expert_up[0]
    down_matrix = expert_down[0]
    experts = lax.axis_size("ep")
    choose = (routes[:, :, None] == jnp.arange(experts, dtype=jnp.int32)[None, None, :]).astype(
        jnp.float32
    )
    weight_table = jnp.sum(route_weights[:, :, None] * choose, axis=1)
    expert_input = lax.all_gather(normed_block, "ep", axis=0, tiled=True)
    table_all = lax.all_gather(weight_table, "ep", axis=0, tiled=True)
    summed = (
        lax.psum(local_product(expert_input, gate_matrix).astype(jnp.bfloat16), "tp").astype(
            jnp.float32
        ),
        lax.psum(local_product(expert_input, up_matrix).astype(jnp.bfloat16), "tp").astype(
            jnp.float32
        ),
        lax.psum(local_product(normed_block, shared_gate).astype(jnp.bfloat16), "tp").astype(
            jnp.float32
        ),
        lax.psum(local_product(normed_block, shared_up).astype(jnp.bfloat16), "tp").astype(
            jnp.float32
        ),
    )
    routed_hidden = (jax.nn.silu(summed[0]) * summed[1]).astype(jnp.bfloat16)
    shared_hidden = (jax.nn.silu(summed[2]) * summed[3]).astype(jnp.bfloat16)
    expert_rows = local_product(routed_hidden, down_matrix).astype(jnp.bfloat16)
    shared_out = local_product(shared_hidden, shared_down)
    own_expert = lax.axis_index("ep")
    column = lax.dynamic_slice_in_dim(table_all, own_expert, 1, 1)
    routed = lax.psum_scatter(
        (column * expert_rows.astype(jnp.float32)).astype(jnp.bfloat16),
        "ep",
        scatter_dimension=0,
        tiled=True,
    ).astype(jnp.float32)
    mixture = routed + shared_out
    square_sum = lax.psum(jnp.sum(mixture * mixture, axis=-1, keepdims=True), "tp")
    scale = lax.rsqrt(square_sum / full_width + epsilon)
    return (mixture * scale * out_gain).astype(jnp.bfloat16)


def solution(mesh):
    chips = mesh.shape["ep"] // 2
    if mesh.shape["tp"] == 2 and mesh.shape["ep"] == 8:
        body = functools.partial(fused, chips)
    else:
        body = per_device
    return jax.shard_map(
        body,
        mesh=mesh,
        in_specs=(
            P(("grp", "ep"), "tp"),
            P(("grp", "ep"), None),
            P(("grp", "ep"), None),
            P(),
            P("ep", "tp", None),
            P("ep", "tp", None),
            P("ep", None, "tp"),
            P("tp", None),
            P("tp", None),
            P(None, "tp"),
            P("tp"),
        ),
        out_specs=P(("grp", "ep"), "tp"),
        check_vma=False,
    )
```

profile of v0, /device:TPU:1, one launch (start us, length us, event | category | flops | bytes accessed | tf_op | source)
XLA Modules:
  0.0 99.5 jit_solution(1353192717544122671)
XLA Ops:
  0.0 97.6 %shard_map.109 = bf16[128,2048]{1,0:T(8,128)(2,1)} custom-call(bf16[128,2048]{1,0:T(8,128)(2,1)} %tokens_hbm.1, s32[4,128]{1,0:T(4,128)} %bitcast.6, f32[4,128]{1,0:T(4,128)} %bitcast.7, f32[1,4096]{1,0:T(1,128)} %bitcast.4, bf16[1,2048,1024]{2,1,0:T(8,128)(2,1)} %gate_hbm.1, bf16[1,2048,1024]{2,1,0:T(8,128)(2,1)} %up_hbm.1, ...), custom_call_target="tpu_custom_call" | custom-call | tf_op jit(solution)/shard_map/pallas_call | solution.py:487
  97.6 1.9 %copy.13 = bf16[128,2048]{1,0:T(8,128)(2,1)} copy(bf16[128,2048]{1,0:T(8,128)(2,1)} %shard_map.109) | data formatting | bytes 1048576
where the time goes:
time: 99.6 us; the launch traced here: 99.5 us
  Pallas kernels  97.6 us (98%)
  local copies, waits for them, and re-layouts  1.88 us (2%)
    pallas_call x1, Pallas kernels, fused(): pl.pallas_call(functools.partial(fused_kernel, chips), out_shape=jax.Shap...  97.6 us

commit v1 on v0

--- a/solution.py
+++ b/solution.py
@@ -9,16 +9,21 @@
 
 epsilon = 1e-06
 MESH = pl.DeviceIdType.MESH
-TABLE = 128
 
 
 def plan(chips):
     ring = [mask for mask in range(2, chips)]
-    first = [(0, 0), (0, 1), (1, 0)]
-    steps = first + [(mask, 0) for mask in ring] + [(mask, 1) for mask in ring] + [(1, 1), None]
+    first = [(0, "own"), (1, 0)]
+    last = [(1, 1), (0, "other"), None]
+    steps = first + [(mask, 0) for mask in ring] + [(mask, 1) for mask in ring] + last
     relays = [[steps.index((distance, 0)), steps.index((max(distance, 2), 1))] for distance in range(1, chips)]
     relays[0][1] -= 1
     return steps, relays
+
+
+def order(entry, core):
+    mask, lane = (0, "own") if entry is None else entry
+    return mask, core if lane == "own" else 1 - core if lane == "other" else lane
 
 
 def pick(index, table):
@@ -51,7 +56,6 @@
     shared_down_hbm,
     out_gain_hbm,
     out_ref,
-    tokens_ref,
     routes_ref,
     weights_ref,
     norm_gain_ref,
@@ -60,6 +64,7 @@
     up,
     down,
     held,
+    source,
     part_out,
     part_in,
     part_own,
@@ -73,7 +78,10 @@
     mixture,
     square_out,
     square_in,
+    info,
     load_sem,
+    info_send,
+    info_recv,
     square_send,
     square_recv,
     gather_send,
@@ -88,15 +96,15 @@
     far_send,
     far_recv,
 ):
-    rows, width = tokens_ref.shape
+    rows, width = mixture.shape
     experts = 2 * chips
     units = gate.shape[2]
     half = units // 2
     steps, relays = plan(chips)
     count = len(steps)
-    masks = [0 if s is None else s[0] for s in steps]
-    lanes = [0 if s is None else s[1] for s in steps]
-    shared_at = steps.index(None)
+    masks = [order(entry, 0)[0] for entry in steps]
+    lanes = [[order(entry, side)[1] for entry in steps] for side in range(2)]
+    shared_at, other_at = steps.index(None), steps.index((0, "other"))
 
     ep = lax.axis_index("ep")
     tp = lax.axis_index("tp")
@@ -105,36 +113,40 @@
     partner = {"ep": chip * 2 + other_core}
     across = {"tp": 1 - tp}
 
-    loads = [
-        pltpu.make_async_copy(source, target, load_sem.at[i])
-        for i, (source, target) in enumerate(
+    away = pl.ds(pl.multiple_of((1 - tp) * half, half), half)
+    near = pl.ds(pl.multiple_of(tp * half, half), half)
+    features = pl.ds(pl.multiple_of(tp * width, width), width)
+    loads = {
+        name: pltpu.make_async_copy(source, target, load_sem.at[i])
+        for i, (name, source, target) in enumerate(
             [
-                (gate_hbm.at[0], gate.at[0]),
-                (up_hbm.at[0], up.at[0]),
-                (shared_gate_hbm, gate.at[1]),
-                (shared_up_hbm, up.at[1]),
-                (down_hbm.at[0], down.at[0]),
-                (shared_down_hbm, down.at[1]),
-                (tokens_hbm, tokens_ref),
-                (routes_hbm, routes_ref),
-                (weights_hbm, weights_ref),
-                (norm_gain_hbm, norm_gain_ref),
-                (out_gain_hbm, out_gain_ref),
+                ("tokens", tokens_hbm, held.at[ep]),
+                ("norm_gain", norm_gain_hbm.at[:, features], norm_gain_ref),
+                ("gate_away", gate_hbm.at[0, :, away], gate.at[0, :, away]),
+                ("up_away", up_hbm.at[0, :, away], up.at[0, :, away]),
+                ("gate_near", gate_hbm.at[0, :, near], gate.at[0, :, near]),
+                ("up_near", up_hbm.at[0, :, near], up.at[0, :, near]),
+                ("routes", routes_hbm, routes_ref),
+                ("weights", weights_hbm, weights_ref),
+                ("down", down_hbm.at[0], down.at[0]),
+                ("shared_gate", shared_gate_hbm, gate.at[1]),
+                ("shared_up", shared_up_hbm, up.at[1]),
+                ("shared_down", shared_down_hbm, down.at[1]),
+                ("out_gain", out_gain_hbm, out_gain_ref),
             ]
         )
-    ]
-    for load in loads[6:] + loads[:2]:
+    }
+    for load in loads.values():
         load.start()
 
     barrier = pltpu.get_barrier_semaphore()
-    for shift in range(1, chips):
+    for shift in range(1, experts):
         pl.semaphore_signal(
             barrier,
             inc=1,
-            device_id={"ep": lax.rem(chip + shift, chips) * 2 + core},
+            device_id={"ep": lax.rem(ep + shift, experts)},
             device_id_type=MESH,
         )
-    pl.semaphore_signal(barrier, inc=1, device_id=partner, device_id_type=MESH)
     pl.semaphore_signal(barrier, inc=1, device_id=across, device_id_type=MESH)
 
     def remote(source, target, send, recv, device):
@@ -156,6 +168,18 @@
             across,
         )
 
+    def info_copy(shift):
+        return remote(
+            info.at[ep],
+            info.at[ep],
+            info_send.at[shift],
+            info_recv.at[ep],
+            {"ep": lax.rem(ep + shift, experts)},
+        )
+
+    def info_arrival(block):
+        return remote(info.at[block], info.at[block], info_send.at[0], info_recv.at[block], partner)
+
     def gather_copy(origin, way):
         slot = held.at[origin * 2 + core]
         device = ({"ep": (chip - 1) * 2 + core}, {"ep": (chip + 1) * 2 + core}, partner)[way]
@@ -216,30 +240,11 @@
     def unpack(row):
         return jnp.transpose(jnp.broadcast_to(row[:1], (128, rows)))[:, :1]
 
-    for load in loads[6:]:
-        load.wait()
-    token_float = tokens_ref[...].astype(jnp.float32)
+    loads["tokens"].wait()
+    token_float = held[ep].astype(jnp.float32)
     own_square = jnp.sum(token_float * token_float, axis=-1, keepdims=True)
     square_out[0] = pack(own_square)
-    pl.semaphore_wait(barrier, chips + 1)
-    square_copy(0).start()
-    lane_ids = lax.broadcasted_iota(jnp.int32, (rows, TABLE), 1)
-    expert_ids = lax.broadcasted_iota(jnp.int32, (TABLE, rows), 0)
-    table = jnp.zeros((TABLE, rows), jnp.float32)
-    for choice in range(routes_ref.shape[0]):
-        named = routes_ref[choice : choice + 1, :]
-        match = (expert_ids == named) | (expert_ids == named + experts)
-        table = table + jnp.where(match, weights_ref[choice : choice + 1, :], 0.0)
-    table = jnp.transpose(table)
-    coarse = table.astype(jnp.bfloat16).astype(jnp.float32)
-    held[ep, :, width:] = jnp.where(lane_ids < experts, table, table - coarse).astype(jnp.bfloat16)
-    mixture[...] = jnp.zeros_like(mixture)
-    square_copy(0).wait_recv()
-    square = own_square + unpack(square_in[0])
-    gain = norm_gain_ref[:, pl.ds(pl.multiple_of(tp * width, width), width)]
-    held[ep, :, :width] = (
-        tokens_ref[...].astype(jnp.float32) * lax.rsqrt(square / (2 * width) + epsilon) * gain
-    ).astype(jnp.bfloat16)
+    pl.semaphore_wait(barrier, experts)
 
     def send_outward():
         @pl.when(chip > 0)
@@ -250,29 +255,43 @@
         def _():
             gather_copy(chip, 1).start()
 
+    pl.when(core == 0)(send_outward)
     gather_copy(chip, 2).start()
-    pl.when(core == 0)(send_outward)
+    square_copy(0).start()
+    loads["norm_gain"].wait()
+
+    def share_info():
+        loads["routes"].wait()
+        loads["weights"].wait()
+        expert_ids = lax.broadcasted_iota(jnp.int32, (experts, rows), 0)
+        table = jnp.zeros((experts, rows), jnp.float32)
+        for choice in range(routes_ref.shape[0]):
+            match = expert_ids == routes_ref[choice : choice + 1, :]
+            table = table + jnp.where(match, weights_ref[choice : choice + 1, :], 0.0)
+        info[ep, :experts] = table
+        square_copy(0).wait_recv()
+        square = square_out[0] + square_in[0]
+        info[ep, experts:] = lax.rsqrt(square / (2 * width) + epsilon)
+        for shift in range(1, experts):
+            info_copy(shift).start()
 
     def locate(k):
         origin = exclusive_or(chip, pick(k, masks), chips)
-        lane = pick(k, lanes)
+        lane = jnp.where(core == 0, pick(k, lanes[0]), pick(k, lanes[1]))
         return origin, lane
+
+    def block_of(k):
+        origin, lane = locate(k)
+        return jnp.where(k == shared_at, ep, origin * 2 + lane)
 
     def first_stage(k):
         origin, lane = locate(k)
         is_shared = k == shared_at
 
-        @pl.when(k == 0)
-        def _():
-            loads[0].wait()
-            loads[1].wait()
-            for load in loads[2:6]:
-                load.start()
-
         @pl.when(is_shared)
         def _():
-            loads[2].wait()
-            loads[3].wait()
+            loads["shared_gate"].wait()
+            loads["shared_up"].wait()
 
         for index, positions in enumerate(relays):
             distance = index + 1
@@ -300,26 +319,34 @@
         def _():
             pair_gather_arrival(origin).wait_recv()
 
-        block = jnp.where(is_shared, ep, origin * 2 + lane)
+        block = block_of(k)
         kind = jnp.where(is_shared, 1, 0)
-        source = held[block, :, :width]
-        away = pl.ds(pl.multiple_of((1 - tp) * half, half), half)
-        near = pl.ds(pl.multiple_of(tp * half, half), half)
-        for which, matrix in enumerate((gate, up)):
+        source[...] = (held[block].astype(jnp.float32) * norm_gain_ref[...]).astype(jnp.bfloat16)
+        for which, matrix, name in ((0, gate, "gate_away"), (1, up, "up_away")):
+            pl.when(k == 0)(loads[name].wait)
             part_out[k, which] = jnp.dot(
-                source, matrix[kind, :, away], preferred_element_type=jnp.float32
+                source[...], matrix[kind, :, away], preferred_element_type=jnp.float32
             ).astype(jnp.bfloat16)
             part_copy(k, which).start()
-        for which, matrix in enumerate((gate, up)):
+        for which, matrix, name in ((0, gate, "gate_near"), (1, up, "up_near")):
+            pl.when(k == 0)(loads[name].wait)
             part_own[k, which] = jnp.dot(
-                source, matrix[kind, :, near], preferred_element_type=jnp.float32
+                source[...], matrix[kind, :, near], preferred_element_type=jnp.float32
             ).astype(jnp.bfloat16)
 
     def second_stage(k):
+        block = block_of(k)
+
+        @pl.when(block != ep)
+        def _():
+            info_arrival(block).wait_recv()
+
+        scale = unpack(info[block, experts : experts + 1])
         part_copy(k, 0).wait_recv()
         part_copy(k, 1).wait_recv()
         gate_sum = part_own[k, 0].astype(jnp.float32) + part_in[k, 0].astype(jnp.float32)
         up_sum = part_own[k, 1].astype(jnp.float32) + part_in[k, 1].astype(jnp.float32)
+        gate_sum, up_sum = gate_sum * scale, up_sum * scale
         hidden[k, tp] = (jax.nn.silu(gate_sum) * up_sum).astype(jnp.bfloat16)
         hidden_copy(k, tp).start()
 
@@ -327,32 +354,29 @@
         origin, lane = locate(k)
         is_shared = k == shared_at
 
-        @pl.when(k == 0)
-        def _():
-            loads[4].wait()
-            loads[5].wait()
-
-        hidden_copy(k, 1 - tp).wait_recv()
-        block = jnp.where(is_shared, ep, origin * 2 + lane)
+        pl.when(k == 0)(loads["down"].wait)
+        pl.when(is_shared)(loads["shared_down"].wait)
         kind = jnp.where(is_shared, 1, 0)
-        chosen = (lane_ids == ep) | (lane_ids == ep + experts)
-        scale = jnp.sum(
-            jnp.where(chosen, held[block, :, width:].astype(jnp.float32), 0.0),
-            axis=-1,
-            keepdims=True,
-        )
         tile = width // 4
 
-        def tile_step(i, carry):
+        def own_step(i, carry):
             columns = pl.ds(pl.multiple_of(i * tile, tile), tile)
             product[:, columns] = jnp.dot(
-                hidden[k, 0], down[kind, :half, columns], preferred_element_type=jnp.float32
-            ) + jnp.dot(
-                hidden[k, 1], down[kind, half:, columns], preferred_element_type=jnp.float32
+                hidden[k, tp], down[kind, near, columns], preferred_element_type=jnp.float32
             )
             return carry
 
-        lax.fori_loop(0, 4, tile_step, 0)
+        def other_step(i, carry):
+            columns = pl.ds(pl.multiple_of(i * tile, tile), tile)
+            product[:, columns] += jnp.dot(
+                hidden[k, 1 - tp], down[kind, away, columns], preferred_element_type=jnp.float32
+            )
+            return carry
+
+        lax.fori_loop(0, 4, own_step, 0)
+        scale = unpack(info[block_of(k), pl.ds(ep, 1)])
+        hidden_copy(k, 1 - tp).wait_recv()
+        lax.fori_loop(0, 4, other_step, 0)
 
         def weighted():
             return product[...].astype(jnp.bfloat16).astype(jnp.float32) * scale
@@ -366,21 +390,25 @@
             pair_out[origin] = weighted().astype(jnp.bfloat16)
             pair_copy(origin).start()
 
-        @pl.when((k != shared_at) & (lane == core))
+        @pl.when(k == 0)
+        def _():
+            mixture[...] = weighted()
+
+        @pl.when((k != 0) & (k != shared_at) & (lane == core))
         def _():
             waiting[...] = weighted()
 
     def fourth_stage(k):
         origin, lane = locate(k)
 
-        @pl.when((k != shared_at) & (lane == core))
+        @pl.when(k == other_at)
+        def _():
+            pair_copy(chip).wait_recv()
+            mixture[...] += pair_in[chip].astype(jnp.float32)
+
+        @pl.when((k != 0) & (k != shared_at) & (lane == core))
         def _():
             pair_copy(origin).wait_recv()
-
-            @pl.when(origin == chip)
-            def _():
-                mixture[...] += waiting[...] + pair_in[origin].astype(jnp.float32)
-
             mask = pick(k, masks)
 
             @pl.when(mask == 3)
@@ -388,18 +416,18 @@
                 far_arrival(opposite).wait_recv()
                 waiting[...] += far_in[opposite].astype(jnp.float32)
 
-            @pl.when(origin != chip)
-            def _():
-                far_out[origin] = (waiting[...] + pair_in[origin].astype(jnp.float32)).astype(
-                    jnp.bfloat16
-                )
-                far_copy(mask, origin).start()
+            far_out[origin] = (waiting[...] + pair_in[origin].astype(jnp.float32)).astype(
+                jnp.bfloat16
+            )
+            far_copy(mask, origin).start()
 
     def body(i, carry):
         @pl.when(i < count)
         def _():
             first_stage(i)
 
+        pl.when(i == 0)(share_info)
+
         @pl.when(i >= 3)
         def _():
             fourth_stage(i - 3)
@@ -408,7 +436,7 @@
         def _():
             second_stage(i - 1)
 
-        @pl.when((i == 2) & (core == 1))
+        @pl.when((i == 1) & (core == 1))
         def _():
             send_outward()
 
@@ -428,6 +456,7 @@
     own_total = jnp.sum(mixed * mixed, axis=-1, keepdims=True)
     square_out[1] = pack(own_total)
     square_copy(1).start()
+    loads["out_gain"].wait()
     square_copy(1).wait_recv()
     total = own_total + unpack(square_in[1])
     out_ref[...] = (
@@ -436,6 +465,8 @@
 
     square_copy(0).wait_send()
     square_copy(1).wait_send()
+    for shift in range(1, experts):
+        info_copy(shift).wait_send()
     for origin in range(chips):
         gather_copy(origin, 2).wait_send()
         pair_copy(origin).wait_send()
@@ -486,19 +517,19 @@
     dma = pltpu.SemaphoreType.DMA
     return pl.pallas_call(
         functools.partial(fused_kernel, chips),
-        out_shape=jax.ShapeDtypeStruct((rows, width), bf16),
+        out_shape=pltpu.VMEM((rows, width), bf16),
         in_specs=[hbm] * 11,
         out_specs=vmem,
         scratch_shapes=[
-            pltpu.VMEM((rows, width), bf16),
             pltpu.VMEM((choices, rows), jnp.int32),
             pltpu.VMEM((choices, rows), f32),
-            pltpu.VMEM((1, norm_gain.shape[0]), f32),
+            pltpu.VMEM((1, width), f32),
             pltpu.VMEM((1, width), f32),
             pltpu.VMEM((2, width, units), bf16),
             pltpu.VMEM((2, width, units), bf16),
             pltpu.VMEM((2, units, width), bf16),
-            pltpu.VMEM((2 * chips, rows, width + TABLE), bf16),
+            pltpu.VMEM((2 * chips, rows, width), bf16),
+            pltpu.VMEM((rows, width), bf16),
             pltpu.VMEM((count, 2, rows, half), bf16),
             pltpu.VMEM((count, 2, rows, half), bf16),
             pltpu.VMEM((count, 2, rows, half), bf16),
@@ -512,7 +543,10 @@
             pltpu.VMEM((rows, width), f32),
             pltpu.VMEM((2, 8, rows), f32),
             pltpu.VMEM((2, 8, rows), f32),
-            dma((11,)),
+            pltpu.VMEM((2 * chips, 2 * chips + 8, rows), f32),
+            dma((13,)),
+            dma((2 * chips,)),
+            dma((2 * chips,)),
             dma((2,)),
             dma((2,)),
             dma((chips, 3)),

time: 99.6 us -> 98.9 us (level)
  local copies, waits for them, and re-layouts: 1.88 us -> 0.8 us
    unnamed x1, local copies, waits for them, and re-layouts: 1.88 us -> 0.8 us
where the time goes in v1:
time: 98.9 us; the launch traced here: 97.9 us
  Pallas kernels  97.1 us (98%)
    pallas_call x1, Pallas kernels, fused(): pl.pallas_call(functools.partial(fused_kernel, chips), out_shape=pltpu.VM...  97.1 us

profile of v1, /device:TPU:1, one launch (start us, length us, event | category | flops | bytes accessed | tf_op | source)
XLA Modules:
  0.0 97.9 jit_solution(11502002312010711684)
XLA Ops:
  0.0 97.1 %shard_map.109 = bf16[128,2048]{1,0:T(8,128)(2,1)S(1)} custom-call(bf16[128,2048]{1,0:T(8,128)(2,1)} %tokens_hbm.1, s32[4,128]{1,0:T(4,128)} %bitcast.6, f32[4,128]{1,0:T(4,128)} %bitcast.7, f32[1,4096]{1,0:T(1,128)} %bitcast.4, bf16[1,2048,1024]{2,1,0:T(8,128)(2,1)} %gate_hbm.1, bf16[1,2048,1024]{2,1,0:T(8,128)(2,1)} %up_hbm.1, ...), custom_call_target="tpu_custom_call" | custom-call | tf_op jit(solution)/shard_map/pallas_call | solution.py:518
  97.2 0.8 copy.13

commit v2 on v1

--- a/solution.py
+++ b/solution.py
@@ -11,19 +11,18 @@
 MESH = pl.DeviceIdType.MESH
 
 
-def plan(chips):
-    ring = [mask for mask in range(2, chips)]
-    first = [(0, "own"), (1, 0)]
-    last = [(1, 1), (0, "other"), None]
-    steps = first + [(mask, 0) for mask in ring] + [(mask, 1) for mask in ring] + last
-    relays = [[steps.index((distance, 0)), steps.index((max(distance, 2), 1))] for distance in range(1, chips)]
-    relays[0][1] -= 1
-    return steps, relays
-
-
-def order(entry, core):
-    mask, lane = (0, "own") if entry is None else entry
-    return mask, core if lane == "own" else 1 - core if lane == "other" else lane
+NEAR, MIDDLE, FAR = range(3)
+STEPS = (
+    "own",
+    (NEAR, 0),
+    (MIDDLE, 0),
+    (FAR, 0),
+    (FAR, 1),
+    (MIDDLE, 1),
+    (NEAR, 1),
+    "other",
+    "shared",
+)
 
 
 def pick(index, table):
@@ -78,6 +77,7 @@
     mixture,
     square_out,
     square_in,
+    info_out,
     info,
     load_sem,
     info_send,
@@ -100,11 +100,13 @@
     experts = 2 * chips
     units = gate.shape[2]
     half = units // 2
-    steps, relays = plan(chips)
-    count = len(steps)
-    masks = [order(entry, 0)[0] for entry in steps]
-    lanes = [[order(entry, side)[1] for entry in steps] for side in range(2)]
-    shared_at, other_at = steps.index(None), steps.index((0, "other"))
+    count = len(STEPS)
+    slots = [step[0] if isinstance(step, tuple) else NEAR for step in STEPS]
+    lanes = [
+        [side if step == "own" else 1 - side if step == "other" else step[1] if isinstance(step, tuple) else side for step in STEPS]
+        for side in range(2)
+    ]
+    shared_at, other_at = STEPS.index("shared"), STEPS.index("other")
 
     ep = lax.axis_index("ep")
     tp = lax.axis_index("tp")
@@ -170,7 +172,7 @@
 
     def info_copy(shift):
         return remote(
-            info.at[ep],
+            info_out.at[shift],
             info.at[ep],
             info_send.at[shift],
             info_recv.at[ep],
@@ -214,23 +216,31 @@
         )
 
     beside, opposite, beyond = (exclusive_or(chip, mask, chips) for mask in (1, 2, 3))
-
-    def far_copy(mask, origin):
-        slot = jnp.where(mask == 2, beyond, chip)
-        return remote(
-            far_out.at[origin],
-            far_in.at[slot],
-            far_send.at[origin],
-            far_recv.at[slot],
-            {"ep": jnp.where(mask == 3, beyond, beside) * 2 + core},
-        )
-
-    def far_arrival(slot):
+    outer = (chip == 0) | (chip == chips - 1)
+    inner = jnp.logical_not(outer)
+
+    def origin_of(slot):
+        middle, far = jnp.where(outer, opposite, beyond), jnp.where(outer, beyond, opposite)
+        return jnp.where(slot == NEAR, beside, jnp.where(slot == MIDDLE, middle, far))
+
+    def far_copy(slot):
+        direct = outer | (slot == NEAR)
+        place = jnp.where(direct, slot, FAR + 1)
+        target = jnp.where(direct, beside, origin_of(slot))
         return remote(
             far_out.at[slot],
-            far_in.at[slot],
+            far_in.at[place],
             far_send.at[slot],
-            far_recv.at[slot],
+            far_recv.at[place],
+            {"ep": target * 2 + core},
+        )
+
+    def far_arrival(place):
+        return remote(
+            far_out.at[0],
+            far_in.at[place],
+            far_send.at[0],
+            far_recv.at[place],
             {"ep": beside * 2 + core},
         )
 
@@ -263,20 +273,89 @@
     def share_info():
         loads["routes"].wait()
         loads["weights"].wait()
-        expert_ids = lax.broadcasted_iota(jnp.int32, (experts, rows), 0)
-        table = jnp.zeros((experts, rows), jnp.float32)
-        for choice in range(routes_ref.shape[0]):
-            match = expert_ids == routes_ref[choice : choice + 1, :]
-            table = table + jnp.where(match, weights_ref[choice : choice + 1, :], 0.0)
-        info[ep, :experts] = table
         square_copy(0).wait_recv()
         square = square_out[0] + square_in[0]
-        info[ep, experts:] = lax.rsqrt(square / (2 * width) + epsilon)
-        for shift in range(1, experts):
-            info_copy(shift).start()
+        scale = lax.rsqrt(square / (2 * width) + epsilon)
+        first_row = lax.broadcasted_iota(jnp.int32, scale.shape, 0) == 0
+        for shift in range(experts):
+            named = routes_ref[...] == lax.rem(ep + shift, experts)
+            weight = jnp.sum(jnp.where(named, weights_ref[...], 0.0), axis=0, keepdims=True)
+            message = jnp.where(first_row, weight, scale)
+            if shift == 0:
+                info[ep] = message
+            else:
+                info_out[shift] = message
+                info_copy(shift).start()
+
+    def take(origin):
+        gather_copy(origin, 0).wait_recv()
+        gather_copy(origin, 2).start()
+
+    def toward_outer(origin):
+        @pl.when(chip == 1)
+        def _():
+            gather_copy(origin, 0).start()
+
+        @pl.when(chip == chips - 2)
+        def _():
+            gather_copy(origin, 1).start()
+
+    def toward_inner(origin):
+        @pl.when(chip < chips // 2)
+        def _():
+            gather_copy(origin, 1).start()
+
+        @pl.when(chip >= chips // 2)
+        def _():
+            gather_copy(origin, 0).start()
+
+    def relay(distance):
+        @pl.when(chip >= distance)
+        def _():
+            take(chip - distance)
+
+            @pl.when(chip < chips - 1)
+            def _():
+                gather_copy(chip - distance, 1).start()
+
+        @pl.when(chip + distance < chips)
+        def _():
+            take(chip + distance)
+
+            @pl.when(chip > 0)
+            def _():
+                gather_copy(chip + distance, 0).start()
+
+    def second_lane_between(i):
+        @pl.when((i == 1) & outer)
+        def _():
+            toward_inner(chip)
+
+        @pl.when((i == 2) & inner)
+        def _():
+            take(beside)
+            toward_inner(beside)
+            toward_inner(chip)
+
+        @pl.when((i == 4) & inner)
+        def _():
+            take(beyond)
+            toward_outer(beyond)
+            toward_outer(chip)
+
+    def second_lane_after(i):
+        @pl.when((i == 3) & inner)
+        def _():
+            take(opposite)
+            toward_outer(opposite)
+
+        @pl.when((i >= 3) & (i < 6) & outer)
+        def _():
+            take(origin_of(pick(i + 1, slots)))
 
     def locate(k):
-        origin = exclusive_or(chip, pick(k, masks), chips)
+        away_from = origin_of(pick(k, slots))
+        origin = jnp.where((k == 0) | (k >= other_at), chip, away_from)
         lane = jnp.where(core == 0, pick(k, lanes[0]), pick(k, lanes[1]))
         return origin, lane
 
@@ -293,27 +372,8 @@
             loads["shared_gate"].wait()
             loads["shared_up"].wait()
 
-        for index, positions in enumerate(relays):
-            distance = index + 1
-            position = jnp.where(core == 0, positions[0], positions[1])
-
-            @pl.when((k == position) & (chip >= distance))
-            def _(distance=distance):
-                gather_copy(chip - distance, 0).wait_recv()
-                gather_copy(chip - distance, 2).start()
-
-                @pl.when(chip < chips - 1)
-                def _():
-                    gather_copy(chip - distance, 1).start()
-
-            @pl.when((k == position) & (chip + distance < chips))
-            def _(distance=distance):
-                gather_copy(chip + distance, 1).wait_recv()
-                gather_copy(chip + distance, 2).start()
-
-                @pl.when(chip > 0)
-                def _():
-                    gather_copy(chip + distance, 0).start()
+        pl.when((k == 2) & (core == 0) & outer)(functools.partial(relay, 2))
+        pl.when((k == 3) & (core == 0))(functools.partial(relay, 3))
 
         @pl.when((lane != core) & (k != shared_at))
         def _():
@@ -341,7 +401,7 @@
         def _():
             info_arrival(block).wait_recv()
 
-        scale = unpack(info[block, experts : experts + 1])
+        scale = unpack(info[block, 1:2])
         part_copy(k, 0).wait_recv()
         part_copy(k, 1).wait_recv()
         gate_sum = part_own[k, 0].astype(jnp.float32) + part_in[k, 0].astype(jnp.float32)
@@ -350,42 +410,41 @@
         hidden[k, tp] = (jax.nn.silu(gate_sum) * up_sum).astype(jnp.bfloat16)
         hidden_copy(k, tp).start()
 
+    def down_product(k, side, columns):
+        rows_of = pl.ds(pl.multiple_of(side * half, half), half)
+        kind = jnp.where(k == shared_at, 1, 0)
+        return jnp.dot(
+            hidden[k, side], down[kind, rows_of, columns], preferred_element_type=jnp.float32
+        )
+
+    tile = width // 4
+
+    def tiles(step):
+        def tile_step(i, carry):
+            step(pl.ds(pl.multiple_of(i * tile, tile), tile))
+            return carry
+
+        lax.fori_loop(0, 4, tile_step, 0)
+
     def third_stage(k):
         origin, lane = locate(k)
-        is_shared = k == shared_at
-
         pl.when(k == 0)(loads["down"].wait)
-        pl.when(is_shared)(loads["shared_down"].wait)
-        kind = jnp.where(is_shared, 1, 0)
-        tile = width // 4
-
-        def own_step(i, carry):
-            columns = pl.ds(pl.multiple_of(i * tile, tile), tile)
-            product[:, columns] = jnp.dot(
-                hidden[k, tp], down[kind, near, columns], preferred_element_type=jnp.float32
-            )
-            return carry
-
-        def other_step(i, carry):
-            columns = pl.ds(pl.multiple_of(i * tile, tile), tile)
-            product[:, columns] += jnp.dot(
-                hidden[k, 1 - tp], down[kind, away, columns], preferred_element_type=jnp.float32
-            )
-            return carry
-
-        lax.fori_loop(0, 4, own_step, 0)
-        scale = unpack(info[block_of(k), pl.ds(ep, 1)])
+
+        def own_step(columns):
+            product[:, columns] = down_product(k, tp, columns)
+
+        def other_step(columns):
+            product[:, columns] += down_product(k, 1 - tp, columns)
+
+        tiles(own_step)
+        scale = unpack(info[block_of(k), :1])
         hidden_copy(k, 1 - tp).wait_recv()
-        lax.fori_loop(0, 4, other_step, 0)
+        tiles(other_step)
 
         def weighted():
             return product[...].astype(jnp.bfloat16).astype(jnp.float32) * scale
 
-        @pl.when(is_shared)
-        def _():
-            mixture[...] += product[...]
-
-        @pl.when((k != shared_at) & (lane != core))
+        @pl.when(lane != core)
         def _():
             pair_out[origin] = weighted().astype(jnp.bfloat16)
             pair_copy(origin).start()
@@ -394,75 +453,95 @@
         def _():
             mixture[...] = weighted()
 
-        @pl.when((k != 0) & (k != shared_at) & (lane == core))
-        def _():
-            waiting[...] = weighted()
+        @pl.when((k != 0) & (lane == core))
+        def _():
+            waiting[pick(k, slots)] = weighted()
 
     def fourth_stage(k):
         origin, lane = locate(k)
 
-        @pl.when(k == other_at)
-        def _():
-            pair_copy(chip).wait_recv()
-            mixture[...] += pair_in[chip].astype(jnp.float32)
-
-        @pl.when((k != 0) & (k != shared_at) & (lane == core))
-        def _():
+        @pl.when((k != 0) & (lane == core))
+        def _():
+            slot = pick(k, slots)
             pair_copy(origin).wait_recv()
-            mask = pick(k, masks)
-
-            @pl.when(mask == 3)
+            waiting[slot] += pair_in[origin].astype(jnp.float32)
+
+            @pl.when(outer | (slot == NEAR))
             def _():
-                far_arrival(opposite).wait_recv()
-                waiting[...] += far_in[opposite].astype(jnp.float32)
-
-            far_out[origin] = (waiting[...] + pair_in[origin].astype(jnp.float32)).astype(
-                jnp.bfloat16
-            )
-            far_copy(mask, origin).start()
+                far_out[slot] = waiting[slot].astype(jnp.bfloat16)
+
+            @pl.when((outer | (slot == NEAR)) & (k != 1))
+            def _():
+                far_copy(slot).start()
+
+    def fifth_stage(k):
+        slot = pick(k, slots)
+        far_arrival(slot).wait_recv()
+        far_out[slot] = (waiting[slot] + far_in[slot].astype(jnp.float32)).astype(jnp.bfloat16)
+        far_copy(slot).start()
 
     def body(i, carry):
+        @pl.when(i == 1)
+        def _():
+            pl.when(core == 0)(functools.partial(relay, 1))
+            second_stage(0)
+
         @pl.when(i < count)
         def _():
             first_stage(i)
 
+        pl.when(core == 1)(functools.partial(second_lane_between, i))
         pl.when(i == 0)(share_info)
 
         @pl.when(i >= 3)
         def _():
             fourth_stage(i - 3)
 
-        @pl.when((i >= 1) & (i < count + 1))
+        @pl.when((i == 5) & (core == 0))
+        def _():
+            far_copy(NEAR).start()
+
+        @pl.when(inner & jnp.where(core == 0, (i == 7) | (i == 8), (i == 8) | (i == 9)))
+        def _():
+            fifth_stage(i - 5 + core)
+
+        pl.when((i == 2) & (core == 0) & inner)(functools.partial(relay, 2))
+
+        @pl.when((i >= 2) & (i < count + 1))
         def _():
             second_stage(i - 1)
 
-        @pl.when((i == 1) & (core == 1))
-        def _():
-            send_outward()
-
-        @pl.when((i >= 2) & (i < count + 2))
+        pl.when(core == 1)(functools.partial(second_lane_after, i))
+
+        @pl.when(i >= 2)
         def _():
             third_stage(i - 2)
 
         return carry
 
-    lax.fori_loop(0, count + 3, body, 0)
-
-    far_arrival(beside).wait_recv()
-    far_arrival(beyond).wait_recv()
-    mixture[...] += far_in[beside].astype(jnp.float32) + far_in[beyond].astype(jnp.float32)
-
-    mixed = mixture[...]
-    own_total = jnp.sum(mixed * mixed, axis=-1, keepdims=True)
+    lax.fori_loop(0, count + 1, body, 0)
+
+    def shared_own(columns):
+        mixture[:, columns] += down_product(shared_at, tp, columns)
+
+    loads["shared_down"].wait()
+    tiles(shared_own)
+    pair_copy(chip).wait_recv()
+    mixture[...] += pair_in[chip].astype(jnp.float32)
+    far_arrival(NEAR).wait_recv()
+    mixture[...] += far_in[NEAR].astype(jnp.float32)
+    far_arrival(FAR + 1).wait_recv()
+    mixture[...] += far_in[FAR + 1].astype(jnp.float32)
+    hidden_copy(shared_at, 1 - tp).wait_recv()
+    own_total = jnp.zeros((rows, 1), jnp.float32)
+    for start in range(0, width, tile):
+        columns = slice(start, start + tile)
+        mixed = mixture[:, columns] + down_product(shared_at, 1 - tp, columns)
+        mixture[:, columns] = mixed
+        own_total = own_total + jnp.sum(mixed * mixed, axis=-1, keepdims=True)
     square_out[1] = pack(own_total)
     square_copy(1).start()
     loads["out_gain"].wait()
-    square_copy(1).wait_recv()
-    total = own_total + unpack(square_in[1])
-    out_ref[...] = (
-        mixture[...] * lax.rsqrt(total / (2 * width) + epsilon) * out_gain_ref[...]
-    ).astype(jnp.bfloat16)
-
     square_copy(0).wait_send()
     square_copy(1).wait_send()
     for shift in range(1, experts):
@@ -479,9 +558,8 @@
         def _(origin=origin):
             gather_copy(origin, 0).wait_send()
 
-        @pl.when(chip != origin)
-        def _(origin=origin):
-            far_arrival(origin).wait_send()
+    for slot in (NEAR, MIDDLE, FAR):
+        far_copy(slot).wait_send()
 
     def drain(k, carry):
         part_copy(k, 0).wait_send()
@@ -490,6 +568,11 @@
         return carry
 
     lax.fori_loop(0, count, drain, 0)
+    square_copy(1).wait_recv()
+    total = own_total + unpack(square_in[1])
+    out_ref[...] = (
+        mixture[...] * lax.rsqrt(total / (2 * width) + epsilon) * out_gain_ref[...]
+    ).astype(jnp.bfloat16)
 
 
 def fused(
@@ -535,15 +618,16 @@
             pltpu.VMEM((count, 2, rows, half), bf16),
             pltpu.VMEM((count, 2, rows, half), bf16),
             pltpu.VMEM((rows, width), f32),
-            pltpu.VMEM((rows, width), f32),
+            pltpu.VMEM((3, rows, width), f32),
             pltpu.VMEM((chips, rows, width), bf16),
             pltpu.VMEM((chips, rows, width), bf16),
-            pltpu.VMEM((chips, rows, width), bf16),
-            pltpu.VMEM((chips, rows, width), bf16),
+            pltpu.VMEM((3, rows, width), bf16),
+            pltpu.VMEM((4, rows, width), bf16),
             pltpu.VMEM((rows, width), f32),
             pltpu.VMEM((2, 8, rows), f32),
             pltpu.VMEM((2, 8, rows), f32),
-            pltpu.VMEM((2 * chips, 2 * chips + 8, rows), f32),
+            pltpu.VMEM((2 * chips, 8, rows), f32),
+            pltpu.VMEM((2 * chips, 8, rows), f32),
             dma((13,)),
             dma((2 * chips,)),
             dma((2 * chips,)),
@@ -558,8 +642,8 @@
             dma((count,)),
             dma((chips,)),
             dma((chips,)),
-            dma((chips,)),
-            dma((chips,)),
+            dma((3,)),
+            dma((4,)),
         ],
         compiler_params=pltpu.CompilerParams(
             collective_id=0, has_side_effects=True, vmem_limit_bytes=60 * 1024 * 1024

time: 98.9 us -> 94.3 us (0.953)
  Pallas kernels: 97.1 us -> 93.1 us
    pallas_call x1, Pallas kernels: 97.1 us -> 93.1 us  [fused(): pl.pallas_call(functools.partial(fused_kernel, chips), out_shape=pltpu.VM...]
where the time goes in v2:
time: 94.3 us; the launch traced here: 93.9 us
  Pallas kernels  93.1 us (99%)
    pallas_call x1, Pallas kernels, fused(): pl.pallas_call(functools.partial(fused_kernel, chips), out_shape=pltpu.VM...  93.1 us

profile of v2, /device:TPU:1, one launch (start us, length us, event | category | flops | bytes accessed | tf_op | source)
XLA Modules:
  0.0 93.9 jit_solution(11553960559969431901)
XLA Ops:
  0.0 93.1 %shard_map.109 = bf16[128,2048]{1,0:T(8,128)(2,1)S(1)} custom-call(bf16[128,2048]{1,0:T(8,128)(2,1)} %tokens_hbm.1, s32[4,128]{1,0:T(4,128)} %bitcast.6, f32[4,128]{1,0:T(4,128)} %bitcast.7, f32[1,4096]{1,0:T(1,128)} %bitcast.4, bf16[1,2048,1024]{2,1,0:T(8,128)(2,1)} %gate_hbm.1, bf16[1,2048,1024]{2,1,0:T(8,128)(2,1)} %up_hbm.1, ...), custom_call_target="tpu_custom_call" | custom-call | tf_op jit(solution)/shard_map/pallas_call | solution.py:601
  93.1 0.8 copy.13

commit v3 on v2

--- a/solution.py
+++ b/solution.py
@@ -11,7 +11,7 @@
 MESH = pl.DeviceIdType.MESH
 
 
-NEAR, MIDDLE, FAR = range(3)
+NEAR, MIDDLE, FAR, SPARE, MIXTURE = range(5)
 STEPS = (
     "own",
     (NEAR, 0),
@@ -21,7 +21,6 @@
     (MIDDLE, 1),
     (NEAR, 1),
     "other",
-    "shared",
 )
 
 
@@ -69,12 +68,11 @@
     part_own,
     hidden,
     product,
-    waiting,
+    sums,
     pair_out,
     pair_in,
     far_out,
     far_in,
-    mixture,
     square_out,
     square_in,
     info_out,
@@ -96,7 +94,8 @@
     far_send,
     far_recv,
 ):
-    rows, width = mixture.shape
+    rows, width = product.shape
+    mixture = sums.at[MIXTURE]
     experts = 2 * chips
     units = gate.shape[2]
     half = units // 2
@@ -106,7 +105,8 @@
         [side if step == "own" else 1 - side if step == "other" else step[1] if isinstance(step, tuple) else side for step in STEPS]
         for side in range(2)
     ]
-    shared_at, other_at = STEPS.index("shared"), STEPS.index("other")
+    quarter = half // 2
+    other_at, shared_at = count - 1, count
 
     ep = lax.axis_index("ep")
     tp = lax.axis_index("tp")
@@ -206,12 +206,20 @@
             hidden.at[k, side], hidden.at[k, side], hidden_send.at[k], hidden_recv.at[k], across
         )
 
-    def pair_copy(origin):
+    def shared_copy(piece, side):
+        slot = hidden.at[shared_at, side, :, piece * quarter : (piece + 1) * quarter]
+        at = shared_at + piece
+        return remote(slot, slot, hidden_send.at[at], hidden_recv.at[at], across)
+
+    def part_of(piece):
+        return pl.ds(piece * (width // 2), width // 2)
+
+    def pair_copy(origin, piece):
         return remote(
-            pair_out.at[origin],
-            pair_in.at[origin],
-            pair_send.at[origin],
-            pair_recv.at[origin],
+            pair_out.at[origin, :, part_of(piece)],
+            pair_in.at[origin, :, part_of(piece)],
+            pair_send.at[origin, piece],
+            pair_recv.at[origin, piece],
             partner,
         )
 
@@ -223,24 +231,24 @@
         middle, far = jnp.where(outer, opposite, beyond), jnp.where(outer, beyond, opposite)
         return jnp.where(slot == NEAR, beside, jnp.where(slot == MIDDLE, middle, far))
 
-    def far_copy(slot):
+    def far_copy(slot, piece):
         direct = outer | (slot == NEAR)
         place = jnp.where(direct, slot, FAR + 1)
         target = jnp.where(direct, beside, origin_of(slot))
         return remote(
-            far_out.at[slot],
-            far_in.at[place],
-            far_send.at[slot],
-            far_recv.at[place],
+            far_out.at[slot, :, part_of(piece)],
+            far_in.at[place, :, part_of(piece)],
+            far_send.at[slot, piece],
+            far_recv.at[place, piece],
             {"ep": target * 2 + core},
         )
 
-    def far_arrival(place):
+    def far_arrival(place, piece):
         return remote(
-            far_out.at[0],
-            far_in.at[place],
-            far_send.at[0],
-            far_recv.at[place],
+            far_out.at[0, :, part_of(piece)],
+            far_in.at[place, :, part_of(piece)],
+            far_send.at[0, piece],
+            far_recv.at[place, piece],
             {"ep": beside * 2 + core},
         )
 
@@ -248,7 +256,10 @@
         return jnp.transpose(jnp.broadcast_to(column, (rows, 128)))[:8]
 
     def unpack(row):
-        return jnp.transpose(jnp.broadcast_to(row[:1], (128, rows)))[:, :1]
+        return jnp.transpose(jnp.broadcast_to(row[:1], (128, rows)))
+
+    def across_lanes(column, lanes):
+        return jnp.concatenate([column] * (lanes // 128), axis=1)
 
     loads["tokens"].wait()
     token_float = held[ep].astype(jnp.float32)
@@ -326,73 +337,112 @@
             def _():
                 gather_copy(chip + distance, 0).start()
 
-    def second_lane_between(i):
-        @pl.when((i == 1) & outer)
-        def _():
-            toward_inner(chip)
-
+    def second_lane_before(i):
+        @pl.when((i == 4) & inner)
+        def _():
+            take(beyond)
+            toward_outer(beyond)
+            toward_outer(chip)
+
+        @pl.when((i >= 4) & (i < 7) & outer)
+        def _():
+            take(origin_of(pick(i, slots)))
+
+    def second_lane_after(i):
         @pl.when((i == 2) & inner)
         def _():
             take(beside)
             toward_inner(beside)
             toward_inner(chip)
 
-        @pl.when((i == 4) & inner)
-        def _():
-            take(beyond)
-            toward_outer(beyond)
-            toward_outer(chip)
-
-    def second_lane_after(i):
         @pl.when((i == 3) & inner)
         def _():
             take(opposite)
             toward_outer(opposite)
 
-        @pl.when((i >= 3) & (i < 6) & outer)
-        def _():
-            take(origin_of(pick(i + 1, slots)))
-
     def locate(k):
         away_from = origin_of(pick(k, slots))
-        origin = jnp.where((k == 0) | (k >= other_at), chip, away_from)
+        origin = jnp.where((k == 0) | (k == other_at), chip, away_from)
         lane = jnp.where(core == 0, pick(k, lanes[0]), pick(k, lanes[1]))
         return origin, lane
 
     def block_of(k):
         origin, lane = locate(k)
-        return jnp.where(k == shared_at, ep, origin * 2 + lane)
+        return origin * 2 + lane
+
+    def scaled(block):
+        source[...] = (held[block].astype(jnp.float32) * norm_gain_ref[...]).astype(jnp.bfloat16)
+
+    def product_of(matrix, columns):
+        return jnp.dot(
+            source[...], matrix[columns], preferred_element_type=jnp.float32
+        ).astype(jnp.bfloat16)
 
     def first_stage(k):
         origin, lane = locate(k)
-        is_shared = k == shared_at
-
-        @pl.when(is_shared)
-        def _():
-            loads["shared_gate"].wait()
-            loads["shared_up"].wait()
-
         pl.when((k == 2) & (core == 0) & outer)(functools.partial(relay, 2))
         pl.when((k == 3) & (core == 0))(functools.partial(relay, 3))
 
-        @pl.when((lane != core) & (k != shared_at))
+        @pl.when(lane != core)
         def _():
             pair_gather_arrival(origin).wait_recv()
 
-        block = block_of(k)
-        kind = jnp.where(is_shared, 1, 0)
-        source[...] = (held[block].astype(jnp.float32) * norm_gain_ref[...]).astype(jnp.bfloat16)
+        scaled(block_of(k))
         for which, matrix, name in ((0, gate, "gate_away"), (1, up, "up_away")):
             pl.when(k == 0)(loads[name].wait)
-            part_out[k, which] = jnp.dot(
-                source[...], matrix[kind, :, away], preferred_element_type=jnp.float32
-            ).astype(jnp.bfloat16)
+            part_out[k, which] = product_of(matrix.at[0], (slice(None), away))
             part_copy(k, which).start()
         for which, matrix, name in ((0, gate, "gate_near"), (1, up, "up_near")):
             pl.when(k == 0)(loads[name].wait)
-            part_own[k, which] = jnp.dot(
-                source[...], matrix[kind, :, near], preferred_element_type=jnp.float32
-            ).astype(jnp.bfloat16)
+            part_own[k, which] = product_of(matrix.at[0], (slice(None), near))
+
+    def piece_of(side, piece):
+        return pl.ds(pl.multiple_of(side * half + piece * quarter, quarter), quarter)
+
+    def shared_first(piece):
+        if piece == 0:
+            loads["shared_gate"].wait()
+            loads["shared_up"].wait()
+        else:
+            scaled(ep)
+        for side, target in ((1 - tp, part_out), (tp, part_own)):
+            columns = (slice(None), piece_of(side, piece))
+            for which, matrix in enumerate((gate, up)):
+                place = slice(which * quarter, (which + 1) * quarter)
+                target[shared_at, piece, :, place] = product_of(matrix.at[1], columns)
+            if target is part_out:
+                part_copy(shared_at, piece).start()
+
+    def shared_second(piece):
+        scale = across_lanes(unpack(info[ep, 1:2]), half)
+        part_copy(shared_at, piece).wait_recv()
+        total = part_own[shared_at, piece].astype(jnp.float32)
+        total = (total + part_in[shared_at, piece].astype(jnp.float32)) * scale
+        product_out = jax.nn.silu(total[:, :quarter]) * total[:, quarter:]
+        place = slice(piece * quarter, (piece + 1) * quarter)
+        hidden[shared_at, tp, :, place] = product_out.astype(jnp.bfloat16)
+        shared_copy(piece, tp).start()
+
+    def shared_product(piece, side, columns):
+        place = slice(piece * quarter, (piece + 1) * quarter)
+        return jnp.dot(
+            hidden[shared_at, side, :, place],
+            down[1, piece_of(side, piece), columns],
+            preferred_element_type=jnp.float32,
+        )
+
+    def shared_third():
+        loads["shared_down"].wait()
+
+        def own_step(columns):
+            mixture[:, columns] += shared_product(0, tp, columns)
+
+        def other_step(columns):
+            mixture[:, columns] += shared_product(0, 1 - tp, columns)
+
+        tiles(own_step)
+        shared_copy(0, 1 - tp).wait_recv()
+        tiles(other_step)
 
     def second_stage(k):
         block = block_of(k)
@@ -401,7 +451,7 @@
         def _():
             info_arrival(block).wait_recv()
 
-        scale = unpack(info[block, 1:2])
+        scale = across_lanes(unpack(info[block, 1:2]), half)
         part_copy(k, 0).wait_recv()
         part_copy(k, 1).wait_recv()
         gate_sum = part_own[k, 0].astype(jnp.float32) + part_in[k, 0].astype(jnp.float32)
@@ -412,19 +462,18 @@
 
     def down_product(k, side, columns):
         rows_of = pl.ds(pl.multiple_of(side * half, half), half)
-        kind = jnp.where(k == shared_at, 1, 0)
         return jnp.dot(
-            hidden[k, side], down[kind, rows_of, columns], preferred_element_type=jnp.float32
+            hidden[k, side], down[0, rows_of, columns], preferred_element_type=jnp.float32
         )
 
     tile = width // 4
 
-    def tiles(step):
+    def tiles(step, first=0, last=4):
         def tile_step(i, carry):
             step(pl.ds(pl.multiple_of(i * tile, tile), tile))
             return carry
 
-        lax.fori_loop(0, 4, tile_step, 0)
+        lax.fori_loop(first, last, tile_step, 0)
 
     def third_stage(k):
         origin, lane = locate(k)
@@ -433,29 +482,25 @@
         def own_step(columns):
             product[:, columns] = down_product(k, tp, columns)
 
+        keeper = lane == core
+        kept = jnp.where(keeper, jnp.where(k == 0, MIXTURE, pick(k, slots)), SPARE)
+        sent = jnp.where(keeper, chips, origin)
+
         def other_step(columns):
-            product[:, columns] += down_product(k, 1 - tp, columns)
-
-        tiles(own_step)
-        scale = unpack(info[block_of(k), :1])
+            total = product[:, columns] + down_product(k, 1 - tp, columns)
+            weighted = total.astype(jnp.bfloat16).astype(jnp.float32) * scale
+            sums[kept, :, columns] = weighted
+            pair_out[sent, :, columns] = weighted.astype(jnp.bfloat16)
+
+        tiles(own_step, 0, 4)
+        scale = across_lanes(unpack(info[block_of(k), :1]), tile)
         hidden_copy(k, 1 - tp).wait_recv()
-        tiles(other_step)
-
-        def weighted():
-            return product[...].astype(jnp.bfloat16).astype(jnp.float32) * scale
-
-        @pl.when(lane != core)
-        def _():
-            pair_out[origin] = weighted().astype(jnp.bfloat16)
-            pair_copy(origin).start()
-
-        @pl.when(k == 0)
-        def _():
-            mixture[...] = weighted()
-
-        @pl.when((k != 0) & (lane == core))
-        def _():
-            waiting[pick(k, slots)] = weighted()
+        for piece in range(2):
+            tiles(other_step, 2 * piece, 2 * piece + 2)
+
+            @pl.when(lane != core)
+            def _(piece=piece):
+                pair_copy(origin, piece).start()
 
     def fourth_stage(k):
         origin, lane = locate(k)
@@ -463,47 +508,67 @@
         @pl.when((k != 0) & (lane == core))
         def _():
             slot = pick(k, slots)
-            pair_copy(origin).wait_recv()
-            waiting[slot] += pair_in[origin].astype(jnp.float32)
-
-            @pl.when(outer | (slot == NEAR))
-            def _():
-                far_out[slot] = waiting[slot].astype(jnp.bfloat16)
-
-            @pl.when((outer | (slot == NEAR)) & (k != 1))
-            def _():
-                far_copy(slot).start()
+            direct = outer | (slot == NEAR)
+            for piece in range(2):
+                columns = part_of(piece)
+                pair_copy(origin, piece).wait_recv()
+                total = sums[slot, :, columns] + pair_in[origin, :, columns].astype(jnp.float32)
+                sums[slot, :, columns] = total
+                far_out[slot, :, columns] = total.astype(jnp.bfloat16)
+
+                @pl.when(direct & (k != 1))
+                def _(piece=piece):
+                    far_copy(slot, piece).start()
 
     def fifth_stage(k):
         slot = pick(k, slots)
-        far_arrival(slot).wait_recv()
-        far_out[slot] = (waiting[slot] + far_in[slot].astype(jnp.float32)).astype(jnp.bfloat16)
-        far_copy(slot).start()
+        for piece in range(2):
+            columns = part_of(piece)
+            far_arrival(slot, piece).wait_recv()
+            total = sums[slot, :, columns] + far_in[slot, :, columns].astype(jnp.float32)
+            far_out[slot, :, columns] = total.astype(jnp.bfloat16)
+            far_copy(slot, piece).start()
 
     def body(i, carry):
+        pl.when(core == 1)(functools.partial(second_lane_before, i))
+
+        @pl.when(i >= 3)
+        def _():
+            fourth_stage(i - 3)
+
+        @pl.when((i == 6) & (core == 0))
+        def _():
+            far_copy(NEAR, 0).start()
+            far_copy(NEAR, 1).start()
+
         @pl.when(i == 1)
         def _():
             pl.when(core == 0)(functools.partial(relay, 1))
             second_stage(0)
+            pl.when((core == 1) & outer)(functools.partial(toward_inner, chip))
 
         @pl.when(i < count)
         def _():
             first_stage(i)
 
-        pl.when(core == 1)(functools.partial(second_lane_between, i))
-        pl.when(i == 0)(share_info)
-
-        @pl.when(i >= 3)
-        def _():
-            fourth_stage(i - 3)
-
-        @pl.when((i == 5) & (core == 0))
-        def _():
-            far_copy(NEAR).start()
-
-        @pl.when(inner & jnp.where(core == 0, (i == 7) | (i == 8), (i == 8) | (i == 9)))
-        def _():
-            fifth_stage(i - 5 + core)
+        pl.when(core == 1)(functools.partial(second_lane_after, i))
+
+        @pl.when(i == 0)
+        def _():
+            shared_first(0)
+            share_info()
+
+        @pl.when(i == 1)
+        def _():
+            shared_second(0)
+
+        @pl.when(i == count)
+        def _():
+            shared_first(1)
+
+        @pl.when(inner & (core == 1) & ((i == 8) | (i == 9)))
+        def _():
+            fifth_stage(i - 4)
 
         pl.when((i == 2) & (core == 0) & inner)(functools.partial(relay, 2))
 
@@ -511,44 +576,54 @@
         def _():
             second_stage(i - 1)
 
-        pl.when(core == 1)(functools.partial(second_lane_after, i))
+        @pl.when(inner & (core == 0) & ((i == 6) | (i == 7)))
+        def _():
+            fifth_stage(i - 4)
+
+        @pl.when(i == count + 1)
+        def _():
+            shared_second(1)
 
         @pl.when(i >= 2)
         def _():
             third_stage(i - 2)
 
+        pl.when(i == 3)(shared_third)
         return carry
 
-    lax.fori_loop(0, count + 1, body, 0)
+    lax.fori_loop(0, count + 2, body, 0)
 
     def shared_own(columns):
-        mixture[:, columns] += down_product(shared_at, tp, columns)
-
-    loads["shared_down"].wait()
+        mixture[:, columns] += shared_product(1, tp, columns)
+
     tiles(shared_own)
-    pair_copy(chip).wait_recv()
-    mixture[...] += pair_in[chip].astype(jnp.float32)
-    far_arrival(NEAR).wait_recv()
-    mixture[...] += far_in[NEAR].astype(jnp.float32)
-    far_arrival(FAR + 1).wait_recv()
-    mixture[...] += far_in[FAR + 1].astype(jnp.float32)
-    hidden_copy(shared_at, 1 - tp).wait_recv()
+    for piece in range(2):
+        pair_copy(chip, piece).wait_recv()
+        mixture[:, part_of(piece)] += pair_in[chip, :, part_of(piece)].astype(jnp.float32)
+    for place in (FAR + 1, NEAR):
+        for piece in range(2):
+            columns = part_of(piece)
+            far_arrival(place, piece).wait_recv()
+            mixture[:, columns] += far_in[place, :, columns].astype(jnp.float32)
+    shared_copy(1, 1 - tp).wait_recv()
     own_total = jnp.zeros((rows, 1), jnp.float32)
     for start in range(0, width, tile):
         columns = slice(start, start + tile)
-        mixed = mixture[:, columns] + down_product(shared_at, 1 - tp, columns)
+        mixed = mixture[:, columns] + shared_product(1, 1 - tp, columns)
         mixture[:, columns] = mixed
         own_total = own_total + jnp.sum(mixed * mixed, axis=-1, keepdims=True)
     square_out[1] = pack(own_total)
     square_copy(1).start()
     loads["out_gain"].wait()
+    mixture[...] *= out_gain_ref[...]
     square_copy(0).wait_send()
     square_copy(1).wait_send()
     for shift in range(1, experts):
         info_copy(shift).wait_send()
     for origin in range(chips):
         gather_copy(origin, 2).wait_send()
-        pair_copy(origin).wait_send()
+        pair_copy(origin, 0).wait_send()
+        pair_copy(origin, 1).wait_send()
 
         @pl.when((chip >= origin) & (chip < chips - 1))
         def _(origin=origin):
@@ -559,7 +634,8 @@
             gather_copy(origin, 0).wait_send()
 
     for slot in (NEAR, MIDDLE, FAR):
-        far_copy(slot).wait_send()
+        far_copy(slot, 0).wait_send()
+        far_copy(slot, 1).wait_send()
 
     def drain(k, carry):
         part_copy(k, 0).wait_send()
@@ -568,11 +644,13 @@
         return carry
 
     lax.fori_loop(0, count, drain, 0)
+    for piece in range(2):
+        part_copy(shared_at, piece).wait_send()
+        shared_copy(piece, tp).wait_send()
+
     square_copy(1).wait_recv()
-    total = own_total + unpack(square_in[1])
-    out_ref[...] = (
-        mixture[...] * lax.rsqrt(total / (2 * width) + epsilon) * out_gain_ref[...]
-    ).astype(jnp.bfloat16)
+    scale = lax.rsqrt((own_total + unpack(square_in[1])) / (2 * width) + epsilon)
+    out_ref[...] = (mixture[...] * across_lanes(scale, width)).astype(jnp.bfloat16)
 
 
 def fused(
@@ -618,12 +696,11 @@
             pltpu.VMEM((count, 2, rows, half), bf16),
             pltpu.VMEM((count, 2, rows, half), bf16),
             pltpu.VMEM((rows, width), f32),
-            pltpu.VMEM((3, rows, width), f32),
-            pltpu.VMEM((chips, rows, width), bf16),
+            pltpu.VMEM((5, rows, width), f32),
+            pltpu.VMEM((chips + 1, rows, width), bf16),
             pltpu.VMEM((chips, rows, width), bf16),
             pltpu.VMEM((3, rows, width), bf16),
             pltpu.VMEM((4, rows, width), bf16),
-            pltpu.VMEM((rows, width), f32),
             pltpu.VMEM((2, 8, rows), f32),
             pltpu.VMEM((2, 8, rows), f32),
             pltpu.VMEM((2 * chips, 8, rows), f32),
@@ -638,12 +715,12 @@
             dma((chips,)),
             dma((count, 2)),
             dma((count, 2)),
-            dma((count,)),
-            dma((count,)),
-            dma((chips,)),
-            dma((chips,)),
-            dma((3,)),
-            dma((4,)),
+            dma((count + 1,)),
+            dma((count + 1,)),
+            dma((chips, 2)),
+            dma((chips, 2)),
+            dma((3, 2)),
+            dma((4, 2)),
         ],
         compiler_params=pltpu.CompilerParams(
             collective_id=0, has_side_effects=True, vmem_limit_bytes=60 * 1024 * 1024

time: 94.3 us -> 90.2 us (0.957)
  Pallas kernels: 93.1 us -> 89.2 us
    pallas_call x1, Pallas kernels: 93.1 us -> 89.2 us  [fused(): pl.pallas_call(functools.partial(fused_kernel, chips), out_shape=pltpu.VM...]
where the time goes in v3:
time: 90.2 us; the launch traced here: 90 us
  Pallas kernels  89.2 us (99%)
    pallas_call x1, Pallas kernels, fused(): pl.pallas_call(functools.partial(fused_kernel, chips), out_shape=pltpu.VM...  89.2 us

profile of v3, /device:TPU:1, one launch (start us, length us, event | category | flops | bytes accessed | tf_op | source)
XLA Modules:
  0.0 90.0 jit_solution(14649805109038728484)
XLA Ops:
  0.0 89.2 %shard_map.109 = bf16[128,2048]{1,0:T(8,128)(2,1)S(1)} custom-call(bf16[128,2048]{1,0:T(8,128)(2,1)} %tokens_hbm.1, s32[4,128]{1,0:T(4,128)} %bitcast.6, f32[4,128]{1,0:T(4,128)} %bitcast.7, f32[1,4096]{1,0:T(1,128)} %bitcast.4, bf16[1,2048,1024]{2,1,0:T(8,128)(2,1)} %gate_hbm.1, bf16[1,2048,1024]{2,1,0:T(8,128)(2,1)} %up_hbm.1, ...), custom_call_target="tpu_custom_call" | custom-call | tf_op jit(solution)/shard_map/pallas_call | solution.py:679
  89.2 0.8 copy.13

commit v4 on v3

--- a/solution.py
+++ b/solution.py
@@ -118,28 +118,32 @@
     away = pl.ds(pl.multiple_of((1 - tp) * half, half), half)
     near = pl.ds(pl.multiple_of(tp * half, half), half)
     features = pl.ds(pl.multiple_of(tp * width, width), width)
+    groups = [
+        [(tokens_hbm, held.at[ep])],
+        [(norm_gain_hbm.at[:, features], norm_gain_ref)],
+        [(gate_hbm.at[0, :, away], gate.at[0, :, away])],
+        [(up_hbm.at[0, :, away], up.at[0, :, away])],
+        [
+            (gate_hbm.at[0, :, near], gate.at[0, :, near]),
+            (up_hbm.at[0, :, near], up.at[0, :, near]),
+        ],
+        [(routes_hbm, routes_ref), (weights_hbm, weights_ref)],
+        [(shared_gate_hbm, gate.at[1]), (shared_up_hbm, up.at[1])],
+        [(down_hbm.at[0], down.at[0]), (shared_down_hbm, down.at[1])],
+        [(out_gain_hbm, out_gain_ref)],
+    ]
+    wholes = [held.at[ep], norm_gain_ref, gate.at[0, :, away], up.at[0, :, away]]
+    wholes += [gate.at[0], info.at[0], gate, down, out_gain_ref]
+    names = ["tokens", "norm_gain", "gate_away", "up_away", "near", "table"]
+    names += ["shared_in", "down", "out_gain"]
+
     loads = {
-        name: pltpu.make_async_copy(source, target, load_sem.at[i])
-        for i, (name, source, target) in enumerate(
-            [
-                ("tokens", tokens_hbm, held.at[ep]),
-                ("norm_gain", norm_gain_hbm.at[:, features], norm_gain_ref),
-                ("gate_away", gate_hbm.at[0, :, away], gate.at[0, :, away]),
-                ("up_away", up_hbm.at[0, :, away], up.at[0, :, away]),
-                ("gate_near", gate_hbm.at[0, :, near], gate.at[0, :, near]),
-                ("up_near", up_hbm.at[0, :, near], up.at[0, :, near]),
-                ("routes", routes_hbm, routes_ref),
-                ("weights", weights_hbm, weights_ref),
-                ("down", down_hbm.at[0], down.at[0]),
-                ("shared_gate", shared_gate_hbm, gate.at[1]),
-                ("shared_up", shared_up_hbm, up.at[1]),
-                ("shared_down", shared_down_hbm, down.at[1]),
-                ("out_gain", out_gain_hbm, out_gain_ref),
-            ]
-        )
+        name: pltpu.make_async_copy(whole, whole, load_sem.at[i])
+        for i, (name, whole) in enumerate(zip(names, wholes))
     }
-    for load in loads.values():
-        load.start()
+    for i, group in enumerate(groups):
+        for load_from, load_to in group:
+            pltpu.make_async_copy(load_from, load_to, load_sem.at[i]).start()
 
     barrier = pltpu.get_barrier_semaphore()
     for shift in range(1, experts):
@@ -174,42 +178,58 @@
         return remote(
             info_out.at[shift],
             info.at[ep],
-            info_send.at[shift],
-            info_recv.at[ep],
+            info_send.at[0],
+            info_recv.at[0],
             {"ep": lax.rem(ep + shift, experts)},
         )
 
-    def info_arrival(block):
-        return remote(info.at[block], info.at[block], info_send.at[0], info_recv.at[block], partner)
+    def info_all():
+        return remote(
+            info_out.at[1:], info_out.at[1:], info_send.at[0], info_recv.at[0], partner
+        )
 
     def gather_copy(origin, way):
         slot = held.at[origin * 2 + core]
         device = ({"ep": (chip - 1) * 2 + core}, {"ep": (chip + 1) * 2 + core}, partner)[way]
         recv = (pair_gather_recv if way == 2 else gather_recv).at[origin]
-        return remote(slot, slot, gather_send.at[origin, way], recv, device)
+        return remote(slot, slot, gather_send.at[way // 2], recv, device)
 
     def pair_gather_arrival(origin):
         slot = held.at[origin * 2 + other_core]
-        return remote(slot, slot, gather_send.at[origin, 2], pair_gather_recv.at[origin], partner)
+        return remote(slot, slot, gather_send.at[1], pair_gather_recv.at[origin], partner)
 
     def part_copy(k, which):
+        place = lax.rem(k, 3)
         return remote(
             part_out.at[k, which],
             part_in.at[k, which],
-            part_send.at[k, which],
-            part_recv.at[k, which],
+            part_send.at[0],
+            part_recv.at[place],
             across,
         )
 
+    def part_arrival(k):
+        place = lax.rem(k, 3)
+        return remote(
+            part_out.at[k], part_in.at[k], part_send.at[0], part_recv.at[place], across
+        )
+
+    def shared_part_copy(piece):
+        return remote(
+            part_out.at[shared_at, piece],
+            part_in.at[shared_at, piece],
+            part_send.at[0],
+            part_recv.at[3 + piece],
+            across,
+        )
+
     def hidden_copy(k, side):
-        return remote(
-            hidden.at[k, side], hidden.at[k, side], hidden_send.at[k], hidden_recv.at[k], across
-        )
+        slot = hidden.at[k, side]
+        return remote(slot, slot, hidden_send.at[0], hidden_recv.at[lax.rem(k, 4)], across)
 
     def shared_copy(piece, side):
         slot = hidden.at[shared_at, side, :, piece * quarter : (piece + 1) * quarter]
-        at = shared_at + piece
-        return remote(slot, slot, hidden_send.at[at], hidden_recv.at[at], across)
+        return remote(slot, slot, hidden_send.at[0], hidden_recv.at[4 + piece], across)
 
     def part_of(piece):
         return pl.ds(piece * (width // 2), width // 2)
@@ -218,7 +238,7 @@
         return remote(
             pair_out.at[origin, :, part_of(piece)],
             pair_in.at[origin, :, part_of(piece)],
-            pair_send.at[origin, piece],
+            pair_send.at[0],
             pair_recv.at[origin, piece],
             partner,
         )
@@ -238,7 +258,7 @@
         return remote(
             far_out.at[slot, :, part_of(piece)],
             far_in.at[place, :, part_of(piece)],
-            far_send.at[slot, piece],
+            far_send.at[0],
             far_recv.at[place, piece],
             {"ep": target * 2 + core},
         )
@@ -247,7 +267,7 @@
         return remote(
             far_out.at[0, :, part_of(piece)],
             far_in.at[place, :, part_of(piece)],
-            far_send.at[0, piece],
+            far_send.at[0],
             far_recv.at[place, piece],
             {"ep": beside * 2 + core},
         )
@@ -282,8 +302,7 @@
     loads["norm_gain"].wait()
 
     def share_info():
-        loads["routes"].wait()
-        loads["weights"].wait()
+        loads["table"].wait()
         square_copy(0).wait_recv()
         square = square_out[0] + square_in[0]
         scale = lax.rsqrt(square / (2 * width) + epsilon)
@@ -392,8 +411,8 @@
             pl.when(k == 0)(loads[name].wait)
             part_out[k, which] = product_of(matrix.at[0], (slice(None), away))
             part_copy(k, which).start()
-        for which, matrix, name in ((0, gate, "gate_near"), (1, up, "up_near")):
-            pl.when(k == 0)(loads[name].wait)
+        pl.when(k == 0)(loads["near"].wait)
+        for which, matrix in enumerate((gate, up)):
             part_own[k, which] = product_of(matrix.at[0], (slice(None), near))
 
     def piece_of(side, piece):
@@ -401,8 +420,7 @@
 
     def shared_first(piece):
         if piece == 0:
-            loads["shared_gate"].wait()
-            loads["shared_up"].wait()
+            loads["shared_in"].wait()
         else:
             scaled(ep)
         for side, target in ((1 - tp, part_out), (tp, part_own)):
@@ -411,11 +429,11 @@
                 place = slice(which * quarter, (which + 1) * quarter)
                 target[shared_at, piece, :, place] = product_of(matrix.at[1], columns)
             if target is part_out:
-                part_copy(shared_at, piece).start()
+                shared_part_copy(piece).start()
 
     def shared_second(piece):
         scale = across_lanes(unpack(info[ep, 1:2]), half)
-        part_copy(shared_at, piece).wait_recv()
+        shared_part_copy(piece).wait_recv()
         total = part_own[shared_at, piece].astype(jnp.float32)
         total = (total + part_in[shared_at, piece].astype(jnp.float32)) * scale
         product_out = jax.nn.silu(total[:, :quarter]) * total[:, quarter:]
@@ -432,8 +450,6 @@
         )
 
     def shared_third():
-        loads["shared_down"].wait()
-
         def own_step(columns):
             mixture[:, columns] += shared_product(0, tp, columns)
 
@@ -447,13 +463,9 @@
     def second_stage(k):
         block = block_of(k)
 
-        @pl.when(block != ep)
-        def _():
-            info_arrival(block).wait_recv()
-
+        pl.when(k == 1)(info_all().wait_recv)
         scale = across_lanes(unpack(info[block, 1:2]), half)
-        part_copy(k, 0).wait_recv()
-        part_copy(k, 1).wait_recv()
+        part_arrival(k).wait_recv()
         gate_sum = part_own[k, 0].astype(jnp.float32) + part_in[k, 0].astype(jnp.float32)
         up_sum = part_own[k, 1].astype(jnp.float32) + part_in[k, 1].astype(jnp.float32)
         gate_sum, up_sum = gate_sum * scale, up_sum * scale
@@ -618,36 +630,25 @@
     mixture[...] *= out_gain_ref[...]
     square_copy(0).wait_send()
     square_copy(1).wait_send()
-    for shift in range(1, experts):
-        info_copy(shift).wait_send()
-    for origin in range(chips):
-        gather_copy(origin, 2).wait_send()
-        pair_copy(origin, 0).wait_send()
-        pair_copy(origin, 1).wait_send()
-
-        @pl.when((chip >= origin) & (chip < chips - 1))
-        def _(origin=origin):
-            gather_copy(origin, 1).wait_send()
-
-        @pl.when((chip <= origin) & (chip > 0))
-        def _(origin=origin):
-            gather_copy(origin, 0).wait_send()
-
-    for slot in (NEAR, MIDDLE, FAR):
-        far_copy(slot, 0).wait_send()
-        far_copy(slot, 1).wait_send()
-
-    def drain(k, carry):
-        part_copy(k, 0).wait_send()
-        part_copy(k, 1).wait_send()
-        hidden_copy(k, tp).wait_send()
-        return carry
-
-    lax.fori_loop(0, count, drain, 0)
-    for piece in range(2):
-        part_copy(shared_at, piece).wait_send()
-        shared_copy(piece, tp).wait_send()
-
+    info_all().wait_send()
+
+    def sent(whole, sem):
+        pltpu.make_async_copy(whole, whole, sem.at[0]).wait()
+
+    @pl.when(outer)
+    def _():
+        pltpu.make_async_copy(held.at[0], held.at[0], gather_send.at[0]).wait()
+
+    @pl.when(inner)
+    def _():
+        several = held.at[: chips + 1]
+        pltpu.make_async_copy(several, several, gather_send.at[0]).wait()
+
+    pltpu.make_async_copy(held.at[:chips], held.at[:chips], gather_send.at[1]).wait()
+    sent(part_out, part_send)
+    sent(part_out.at[:, 0], hidden_send)
+    sent(pair_in, pair_send)
+    sent(far_out, far_send)
     square_copy(1).wait_recv()
     scale = lax.rsqrt((own_total + unpack(square_in[1])) / (2 * width) + epsilon)
     out_ref[...] = (mixture[...] * across_lanes(scale, width)).astype(jnp.bfloat16)
@@ -705,21 +706,21 @@
             pltpu.VMEM((2, 8, rows), f32),
             pltpu.VMEM((2 * chips, 8, rows), f32),
             pltpu.VMEM((2 * chips, 8, rows), f32),
-            dma((13,)),
-            dma((2 * chips,)),
-            dma((2 * chips,)),
+            dma((9,)),
+            dma((1,)),
+            dma((1,)),
             dma((2,)),
             dma((2,)),
-            dma((chips, 3)),
+            dma((2,)),
             dma((chips,)),
             dma((chips,)),
-            dma((count, 2)),
-            dma((count, 2)),
-            dma((count + 1,)),
-            dma((count + 1,)),
+            dma((1,)),
+            dma((5,)),
+            dma((1,)),
+            dma((6,)),
+            dma((1,)),
             dma((chips, 2)),
-            dma((chips, 2)),
-            dma((3, 2)),
+            dma((1,)),
             dma((4, 2)),
         ],
         compiler_params=pltpu.CompilerParams(

time: 90.2 us -> 89.4 us (level)
  no operation moved by 1% of the time
where the time goes in v4:
time: 89.4 us; the launch traced here: 89.3 us
  Pallas kernels  88.5 us (99%)
    pallas_call x1, Pallas kernels, fused(): pl.pallas_call(functools.partial(fused_kernel, chips), out_shape=pltpu.VM...  88.5 us

profile of v4, /device:TPU:1, one launch (start us, length us, event | category | flops | bytes accessed | tf_op | source)
XLA Modules:
  0.0 89.3 jit_solution(2023788031307791221)
XLA Ops:
  0.0 88.5 %shard_map.109 = bf16[128,2048]{1,0:T(8,128)(2,1)S(1)} custom-call(bf16[128,2048]{1,0:T(8,128)(2,1)} %tokens_hbm.1, s32[4,128]{1,0:T(4,128)} %bitcast.6, f32[4,128]{1,0:T(4,128)} %bitcast.7, f32[1,4096]{1,0:T(1,128)} %bitcast.4, bf16[1,2048,1024]{2,1,0:T(8,128)(2,1)} %gate_hbm.1, bf16[1,2048,1024]{2,1,0:T(8,128)(2,1)} %up_hbm.1, ...), custom_call_target="tpu_custom_call" | custom-call | tf_op jit(solution)/shard_map/pallas_call | solution.py:680
  88.5 0.8 copy.13

commit v5 on v4

--- a/solution.py
+++ b/solution.py
@@ -75,11 +75,11 @@
     far_in,
     square_out,
     square_in,
-    info_out,
     info,
     load_sem,
     info_send,
     info_recv,
+    pair_info_recv,
     square_send,
     square_recv,
     gather_send,
@@ -133,7 +133,7 @@
         [(out_gain_hbm, out_gain_ref)],
     ]
     wholes = [held.at[ep], norm_gain_ref, gate.at[0, :, away], up.at[0, :, away]]
-    wholes += [gate.at[0], info.at[0], gate, down, out_gain_ref]
+    wholes += [gate.at[0], info.at[0, :8], gate, down, out_gain_ref]
     names = ["tokens", "norm_gain", "gate_away", "up_away", "near", "table"]
     names += ["shared_in", "down", "out_gain"]
 
@@ -146,14 +146,19 @@
             pltpu.make_async_copy(load_from, load_to, load_sem.at[i]).start()
 
     barrier = pltpu.get_barrier_semaphore()
-    for shift in range(1, experts):
-        pl.semaphore_signal(
-            barrier,
-            inc=1,
-            device_id={"ep": lax.rem(ep + shift, experts)},
-            device_id_type=MESH,
-        )
-    pl.semaphore_signal(barrier, inc=1, device_id=across, device_id_type=MESH)
+    def greet(device):
+        pl.semaphore_signal(barrier, inc=1, device_id=device, device_id_type=MESH)
+
+    greet(across)
+    greet(partner)
+
+    @pl.when(chip > 0)
+    def _():
+        greet({"ep": (chip - 1) * 2 + core})
+
+    @pl.when(chip < chips - 1)
+    def _():
+        greet({"ep": (chip + 1) * 2 + core})
 
     def remote(source, target, send, recv, device):
         return pltpu.make_async_remote_copy(
@@ -174,25 +179,26 @@
             across,
         )
 
-    def info_copy(shift):
-        return remote(
-            info_out.at[shift],
-            info.at[ep],
-            info_send.at[0],
-            info_recv.at[0],
-            {"ep": lax.rem(ep + shift, experts)},
-        )
-
-    def info_all():
-        return remote(
-            info_out.at[1:], info_out.at[1:], info_send.at[0], info_recv.at[0], partner
-        )
-
-    def gather_copy(origin, way):
+    def ways(way):
+        return ({"ep": (chip - 1) * 2 + core}, {"ep": (chip + 1) * 2 + core}, partner)[way]
+
+    def tokens_copy(origin, way):
         slot = held.at[origin * 2 + core]
-        device = ({"ep": (chip - 1) * 2 + core}, {"ep": (chip + 1) * 2 + core}, partner)[way]
         recv = (pair_gather_recv if way == 2 else gather_recv).at[origin]
-        return remote(slot, slot, gather_send.at[way // 2], recv, device)
+        return remote(slot, slot, gather_send.at[way // 2], recv, ways(way))
+
+    def info_copy(origin, way):
+        slot = info.at[origin * 2 + core]
+        recv = (pair_info_recv if way == 2 else info_recv).at[origin]
+        return remote(slot, slot, info_send.at[way // 2], recv, ways(way))
+
+    def pass_on(origin, way):
+        tokens_copy(origin, way).start()
+        info_copy(origin, way).start()
+
+    def pair_info_arrival(origin):
+        slot = info.at[origin * 2 + other_core]
+        return remote(slot, slot, info_send.at[1], pair_info_recv.at[origin], partner)
 
     def pair_gather_arrival(origin):
         slot = held.at[origin * 2 + other_core]
@@ -285,59 +291,58 @@
     token_float = held[ep].astype(jnp.float32)
     own_square = jnp.sum(token_float * token_float, axis=-1, keepdims=True)
     square_out[0] = pack(own_square)
-    pl.semaphore_wait(barrier, experts)
-
-    def send_outward():
-        @pl.when(chip > 0)
-        def _():
-            gather_copy(chip, 0).start()
-
-        @pl.when(chip < chips - 1)
-        def _():
-            gather_copy(chip, 1).start()
-
-    pl.when(core == 0)(send_outward)
-    gather_copy(chip, 2).start()
+    pl.semaphore_wait(barrier, jnp.where((chip == 0) | (chip == chips - 1), 3, 4))
+
+    def send_outward(copy):
+        @pl.when((core == 0) & (chip > 0))
+        def _():
+            copy(chip, 0).start()
+
+        @pl.when((core == 0) & (chip < chips - 1))
+        def _():
+            copy(chip, 1).start()
+
+        copy(chip, 2).start()
+
+    send_outward(tokens_copy)
     square_copy(0).start()
     loads["norm_gain"].wait()
 
     def share_info():
         loads["table"].wait()
+        expert_ids = lax.broadcasted_iota(jnp.int32, (experts, rows), 0)
+        table = jnp.zeros((experts, rows), jnp.float32)
+        for choice in range(routes_ref.shape[0]):
+            match = expert_ids == routes_ref[choice : choice + 1, :]
+            table = table + jnp.where(match, weights_ref[choice : choice + 1, :], 0.0)
+        info[ep, :experts] = table
         square_copy(0).wait_recv()
         square = square_out[0] + square_in[0]
-        scale = lax.rsqrt(square / (2 * width) + epsilon)
-        first_row = lax.broadcasted_iota(jnp.int32, scale.shape, 0) == 0
-        for shift in range(experts):
-            named = routes_ref[...] == lax.rem(ep + shift, experts)
-            weight = jnp.sum(jnp.where(named, weights_ref[...], 0.0), axis=0, keepdims=True)
-            message = jnp.where(first_row, weight, scale)
-            if shift == 0:
-                info[ep] = message
-            else:
-                info_out[shift] = message
-                info_copy(shift).start()
+        info[ep, experts:] = lax.rsqrt(square / (2 * width) + epsilon)
+        send_outward(info_copy)
 
     def take(origin):
-        gather_copy(origin, 0).wait_recv()
-        gather_copy(origin, 2).start()
+        tokens_copy(origin, 0).wait_recv()
+        info_copy(origin, 0).wait_recv()
+        pass_on(origin, 2)
 
     def toward_outer(origin):
         @pl.when(chip == 1)
         def _():
-            gather_copy(origin, 0).start()
+            pass_on(origin, 0)
 
         @pl.when(chip == chips - 2)
         def _():
-            gather_copy(origin, 1).start()
+            pass_on(origin, 1)
 
     def toward_inner(origin):
         @pl.when(chip < chips // 2)
         def _():
-            gather_copy(origin, 1).start()
+            pass_on(origin, 1)
 
         @pl.when(chip >= chips // 2)
         def _():
-            gather_copy(origin, 0).start()
+            pass_on(origin, 0)
 
     def relay(distance):
         @pl.when(chip >= distance)
@@ -346,7 +351,7 @@
 
             @pl.when(chip < chips - 1)
             def _():
-                gather_copy(chip - distance, 1).start()
+                pass_on(chip - distance, 1)
 
         @pl.when(chip + distance < chips)
         def _():
@@ -354,7 +359,7 @@
 
             @pl.when(chip > 0)
             def _():
-                gather_copy(chip + distance, 0).start()
+                pass_on(chip + distance, 0)
 
     def second_lane_before(i):
         @pl.when((i == 4) & inner)
@@ -407,10 +412,14 @@
             pair_gather_arrival(origin).wait_recv()
 
         scaled(block_of(k))
-        for which, matrix, name in ((0, gate, "gate_away"), (1, up, "up_away")):
-            pl.when(k == 0)(loads[name].wait)
-            part_out[k, which] = product_of(matrix.at[0], (slice(None), away))
-            part_copy(k, which).start()
+        pl.when(k == 0)(loads["gate_away"].wait)
+        part_out[k, 0] = product_of(gate.at[0], (slice(None), away))
+        part_copy(k, 0).start()
+
+    def finish_first_stage(k):
+        pl.when(k == 0)(loads["up_away"].wait)
+        part_out[k, 1] = product_of(up.at[0], (slice(None), away))
+        part_copy(k, 1).start()
         pl.when(k == 0)(loads["near"].wait)
         for which, matrix in enumerate((gate, up)):
             part_own[k, which] = product_of(matrix.at[0], (slice(None), near))
@@ -432,7 +441,7 @@
                 shared_part_copy(piece).start()
 
     def shared_second(piece):
-        scale = across_lanes(unpack(info[ep, 1:2]), half)
+        scale = across_lanes(unpack(info[ep, experts : experts + 1]), half)
         shared_part_copy(piece).wait_recv()
         total = part_own[shared_at, piece].astype(jnp.float32)
         total = (total + part_in[shared_at, piece].astype(jnp.float32)) * scale
@@ -463,8 +472,13 @@
     def second_stage(k):
         block = block_of(k)
 
-        pl.when(k == 1)(info_all().wait_recv)
-        scale = across_lanes(unpack(info[block, 1:2]), half)
+        origin, lane = locate(k)
+
+        @pl.when(lane != core)
+        def _():
+            pair_info_arrival(origin).wait_recv()
+
+        scale = across_lanes(unpack(info[block, experts : experts + 1]), half)
         part_arrival(k).wait_recv()
         gate_sum = part_own[k, 0].astype(jnp.float32) + part_in[k, 0].astype(jnp.float32)
         up_sum = part_own[k, 1].astype(jnp.float32) + part_in[k, 1].astype(jnp.float32)
@@ -505,7 +519,7 @@
             pair_out[sent, :, columns] = weighted.astype(jnp.bfloat16)
 
         tiles(own_step, 0, 4)
-        scale = across_lanes(unpack(info[block_of(k), :1]), tile)
+        scale = across_lanes(unpack(info[block_of(k), pl.ds(ep, 1)]), tile)
         hidden_copy(k, 1 - tp).wait_recv()
         for piece in range(2):
             tiles(other_step, 2 * piece, 2 * piece + 2)
@@ -528,7 +542,7 @@
                 sums[slot, :, columns] = total
                 far_out[slot, :, columns] = total.astype(jnp.bfloat16)
 
-                @pl.when(direct & (k != 1))
+                @pl.when(direct & (outer | (k != 1)))
                 def _(piece=piece):
                     far_copy(slot, piece).start()
 
@@ -542,13 +556,14 @@
             far_copy(slot, piece).start()
 
     def body(i, carry):
+        early, late = i <= 3, (i >= 4) & (i <= count)
         pl.when(core == 1)(functools.partial(second_lane_before, i))
 
-        @pl.when(i >= 3)
-        def _():
-            fourth_stage(i - 3)
-
-        @pl.when((i == 6) & (core == 0))
+        @pl.when(i == 4)
+        def _():
+            fourth_stage(1)
+
+        @pl.when((i == 6) & (core == 0) & inner)
         def _():
             far_copy(NEAR, 0).start()
             far_copy(NEAR, 1).start()
@@ -563,40 +578,52 @@
         def _():
             first_stage(i)
 
+        @pl.when(i == count)
+        def _():
+            shared_first(1)
+
+        @pl.when(early)
+        def _():
+            finish_first_stage(i)
+
         pl.when(core == 1)(functools.partial(second_lane_after, i))
 
         @pl.when(i == 0)
         def _():
+            share_info()
             shared_first(0)
-            share_info()
 
         @pl.when(i == 1)
         def _():
             shared_second(0)
 
-        @pl.when(i == count)
-        def _():
-            shared_first(1)
-
-        @pl.when(inner & (core == 1) & ((i == 8) | (i == 9)))
-        def _():
-            fifth_stage(i - 4)
+        @pl.when(late)
+        def _():
+            third_stage(i - 2)
 
         pl.when((i == 2) & (core == 0) & inner)(functools.partial(relay, 2))
 
-        @pl.when((i >= 2) & (i < count + 1))
+        @pl.when((i >= 2) & (i <= count))
         def _():
             second_stage(i - 1)
 
-        @pl.when(inner & (core == 0) & ((i == 6) | (i == 7)))
-        def _():
-            fifth_stage(i - 4)
+        @pl.when(late)
+        def _():
+            fourth_stage(i - 2)
+
+        @pl.when(late & (i < count))
+        def _():
+            finish_first_stage(i)
+
+        @pl.when(inner & jnp.where(core == 0, (i == 5) | (i == 6), (i == 7) | (i == 8)))
+        def _():
+            fifth_stage(i - 3)
 
         @pl.when(i == count + 1)
         def _():
             shared_second(1)
 
-        @pl.when(i >= 2)
+        @pl.when((i == 2) | (i == 3) | (i == count + 1))
         def _():
             third_stage(i - 2)
 
@@ -630,21 +657,23 @@
     mixture[...] *= out_gain_ref[...]
     square_copy(0).wait_send()
     square_copy(1).wait_send()
-    info_all().wait_send()
 
     def sent(whole, sem):
         pltpu.make_async_copy(whole, whole, sem.at[0]).wait()
 
-    @pl.when(outer)
-    def _():
-        pltpu.make_async_copy(held.at[0], held.at[0], gather_send.at[0]).wait()
-
-    @pl.when(inner)
-    def _():
-        several = held.at[: chips + 1]
-        pltpu.make_async_copy(several, several, gather_send.at[0]).wait()
-
-    pltpu.make_async_copy(held.at[:chips], held.at[:chips], gather_send.at[1]).wait()
+    for whole, sem in ((held, gather_send), (info, info_send)):
+
+        @pl.when(outer)
+        def _(whole=whole, sem=sem):
+            pltpu.make_async_copy(whole.at[0], whole.at[0], sem.at[0]).wait()
+
+        @pl.when(inner)
+        def _(whole=whole, sem=sem):
+            several = whole.at[: chips + 1]
+            pltpu.make_async_copy(several, several, sem.at[0]).wait()
+
+        pltpu.make_async_copy(whole.at[:chips], whole.at[:chips], sem.at[1]).wait()
+
     sent(part_out, part_send)
     sent(part_out.at[:, 0], hidden_send)
     sent(pair_in, pair_send)
@@ -704,11 +733,11 @@
             pltpu.VMEM((4, rows, width), bf16),
             pltpu.VMEM((2, 8, rows), f32),
             pltpu.VMEM((2, 8, rows), f32),
-            pltpu.VMEM((2 * chips, 8, rows), f32),
-            pltpu.VMEM((2 * chips, 8, rows), f32),
+            pltpu.VMEM((2 * chips, 2 * chips + 8, rows), f32),
             dma((9,)),
-            dma((1,)),
-            dma((1,)),
+            dma((2,)),
+            dma((chips,)),
+            dma((chips,)),
             dma((2,)),
             dma((2,)),
             dma((2,)),

time: 89.4 us -> 87.8 us (0.982)
  Pallas kernels: 88.5 us -> 86.5 us
    pallas_call x1, Pallas kernels: 88.5 us -> 86.5 us  [fused(): pl.pallas_call(functools.partial(fused_kernel, chips), out_shape=pltpu.VM...]
where the time goes in v5:
time: 87.8 us; the launch traced here: 87.3 us
  Pallas kernels  86.5 us (99%)
    pallas_call x1, Pallas kernels, fused(): pl.pallas_call(functools.partial(fused_kernel, chips), out_shape=pltpu.VM...  86.5 us

profile of v5, /device:TPU:1, one launch (start us, length us, event | category | flops | bytes accessed | tf_op | source)
XLA Modules:
  0.0 87.3 jit_solution(8063718586215388750)
XLA Ops:
  0.0 86.5 %shard_map.109 = bf16[128,2048]{1,0:T(8,128)(2,1)S(1)} custom-call(bf16[128,2048]{1,0:T(8,128)(2,1)} %tokens_hbm.1, s32[4,128]{1,0:T(4,128)} %bitcast.6, f32[4,128]{1,0:T(4,128)} %bitcast.7, f32[1,4096]{1,0:T(1,128)} %bitcast.4, bf16[1,2048,1024]{2,1,0:T(8,128)(2,1)} %gate_hbm.1, bf16[1,2048,1024]{2,1,0:T(8,128)(2,1)} %up_hbm.1, ...), custom_call_target="tpu_custom_call" | custom-call | tf_op jit(solution)/shard_map/pallas_call | solution.py:709
  86.5 0.8 copy.13

commit v6 on v5

--- a/solution.py
+++ b/solution.py
@@ -278,8 +278,16 @@
             {"ep": beside * 2 + core},
         )
 
-    def pack(column):
-        return jnp.transpose(jnp.broadcast_to(column, (rows, 128)))[:8]
+    def row_squares(values):
+        total = jnp.zeros((rows, 128), jnp.float32)
+        for start in range(0, values.shape[1], 128):
+            chunk = values[:, start : start + 128]
+            total = total + chunk * chunk
+        return total
+
+    def pack(partial):
+        row = jnp.sum(jnp.transpose(partial), axis=0, keepdims=True)
+        return jnp.broadcast_to(row, (8, rows))
 
     def unpack(row):
         return jnp.transpose(jnp.broadcast_to(row[:1], (128, rows)))
@@ -288,9 +296,7 @@
         return jnp.concatenate([column] * (lanes // 128), axis=1)
 
     loads["tokens"].wait()
-    token_float = held[ep].astype(jnp.float32)
-    own_square = jnp.sum(token_float * token_float, axis=-1, keepdims=True)
-    square_out[0] = pack(own_square)
+    square_out[0] = pack(row_squares(held[ep].astype(jnp.float32)))
     pl.semaphore_wait(barrier, jnp.where((chip == 0) | (chip == chips - 1), 3, 4))
 
     def send_outward(copy):
@@ -499,7 +505,7 @@
             step(pl.ds(pl.multiple_of(i * tile, tile), tile))
             return carry
 
-        lax.fori_loop(first, last, tile_step, 0)
+        lax.fori_loop(first, last, tile_step, 0, unroll=last - first == 2)
 
     def third_stage(k):
         origin, lane = locate(k)
@@ -555,6 +561,9 @@
             far_out[slot, :, columns] = total.astype(jnp.bfloat16)
             far_copy(slot, piece).start()
 
+    def shared_own(columns):
+        mixture[:, columns] += shared_product(1, tp, columns)
+
     def body(i, carry):
         early, late = i <= 3, (i >= 4) & (i <= count)
         pl.when(core == 1)(functools.partial(second_lane_before, i))
@@ -622,6 +631,7 @@
         @pl.when(i == count + 1)
         def _():
             shared_second(1)
+            tiles(shared_own)
 
         @pl.when((i == 2) | (i == 3) | (i == count + 1))
         def _():
@@ -632,26 +642,20 @@
 
     lax.fori_loop(0, count + 2, body, 0)
 
-    def shared_own(columns):
-        mixture[:, columns] += shared_product(1, tp, columns)
-
-    tiles(shared_own)
     for piece in range(2):
         pair_copy(chip, piece).wait_recv()
-        mixture[:, part_of(piece)] += pair_in[chip, :, part_of(piece)].astype(jnp.float32)
-    for place in (FAR + 1, NEAR):
-        for piece in range(2):
-            columns = part_of(piece)
-            far_arrival(place, piece).wait_recv()
-            mixture[:, columns] += far_in[place, :, columns].astype(jnp.float32)
+        far_arrival(FAR + 1, piece).wait_recv()
+        far_arrival(NEAR, piece).wait_recv()
     shared_copy(1, 1 - tp).wait_recv()
-    own_total = jnp.zeros((rows, 1), jnp.float32)
+    squares = jnp.zeros((rows, 128), jnp.float32)
     for start in range(0, width, tile):
         columns = slice(start, start + tile)
         mixed = mixture[:, columns] + shared_product(1, 1 - tp, columns)
+        for arrived in (pair_in.at[chip], far_in.at[FAR + 1], far_in.at[NEAR]):
+            mixed = mixed + arrived[:, columns].astype(jnp.float32)
         mixture[:, columns] = mixed
-        own_total = own_total + jnp.sum(mixed * mixed, axis=-1, keepdims=True)
-    square_out[1] = pack(own_total)
+        squares = squares + row_squares(mixed)
+    square_out[1] = pack(squares)
     square_copy(1).start()
     loads["out_gain"].wait()
     mixture[...] *= out_gain_ref[...]
@@ -679,7 +683,7 @@
     sent(pair_in, pair_send)
     sent(far_out, far_send)
     square_copy(1).wait_recv()
-    scale = lax.rsqrt((own_total + unpack(square_in[1])) / (2 * width) + epsilon)
+    scale = lax.rsqrt(unpack(square_out[1] + square_in[1]) / (2 * width) + epsilon)
     out_ref[...] = (mixture[...] * across_lanes(scale, width)).astype(jnp.bfloat16)
 
 

time: 87.8 us -> 86.6 us (0.986)
  no operation moved by 1% of the time
where the time goes in v6:
time: 86.6 us; the launch traced here: 86.5 us
  Pallas kernels  85.7 us (99%)
    pallas_call x1, Pallas kernels, fused(): pl.pallas_call(functools.partial(fused_kernel, chips), out_shape=pltpu.VM...  85.7 us

profile of v6, /device:TPU:1, one launch (start us, length us, event | category | flops | bytes accessed | tf_op | source)
XLA Modules:
  0.0 86.5 jit_solution(11947492444778255897)
XLA Ops:
  0.0 85.7 %shard_map.109 = bf16[128,2048]{1,0:T(8,128)(2,1)S(1)} custom-call(bf16[128,2048]{1,0:T(8,128)(2,1)} %tokens_hbm.1, s32[4,128]{1,0:T(4,128)} %bitcast.6, f32[4,128]{1,0:T(4,128)} %bitcast.7, f32[1,4096]{1,0:T(1,128)} %bitcast.4, bf16[1,2048,1024]{2,1,0:T(8,128)(2,1)} %gate_hbm.1, bf16[1,2048,1024]{2,1,0:T(8,128)(2,1)} %up_hbm.1, ...), custom_call_target="tpu_custom_call" | custom-call | tf_op jit(solution)/shard_map/pallas_call | solution.py:713
  85.7 0.8 copy.13

commit v7 on v6

--- a/solution.py
+++ b/solution.py
@@ -105,21 +105,27 @@
         [side if step == "own" else 1 - side if step == "other" else step[1] if isinstance(step, tuple) else side for step in STEPS]
         for side in range(2)
     ]
-    quarter = half // 2
+    cuts = [0, half // 4, half]
+    spans = [slice(cuts[piece], cuts[piece + 1]) for piece in range(2)]
     other_at, shared_at = count - 1, count
 
     ep = lax.axis_index("ep")
     tp = lax.axis_index("tp")
-    chip, core = lax.div(ep, 2), lax.rem(ep, 2)
+    chip, core = lax.div(ep, 2), 1 - lax.rem(ep, 2)
     other_core = 1 - core
-    partner = {"ep": chip * 2 + other_core}
+    partner = {"ep": chip * 2 + core}
+    me = chip * 2 + core
+
+    def same_core(place):
+        return {"ep": place * 2 + other_core}
+
     across = {"tp": 1 - tp}
 
     away = pl.ds(pl.multiple_of((1 - tp) * half, half), half)
     near = pl.ds(pl.multiple_of(tp * half, half), half)
     features = pl.ds(pl.multiple_of(tp * width, width), width)
     groups = [
-        [(tokens_hbm, held.at[ep])],
+        [(tokens_hbm, held.at[me])],
         [(norm_gain_hbm.at[:, features], norm_gain_ref)],
         [(gate_hbm.at[0, :, away], gate.at[0, :, away])],
         [(up_hbm.at[0, :, away], up.at[0, :, away])],
@@ -132,7 +138,7 @@
         [(down_hbm.at[0], down.at[0]), (shared_down_hbm, down.at[1])],
         [(out_gain_hbm, out_gain_ref)],
     ]
-    wholes = [held.at[ep], norm_gain_ref, gate.at[0, :, away], up.at[0, :, away]]
+    wholes = [held.at[me], norm_gain_ref, gate.at[0, :, away], up.at[0, :, away]]
     wholes += [gate.at[0], info.at[0, :8], gate, down, out_gain_ref]
     names = ["tokens", "norm_gain", "gate_away", "up_away", "near", "table"]
     names += ["shared_in", "down", "out_gain"]
@@ -154,11 +160,11 @@
 
     @pl.when(chip > 0)
     def _():
-        greet({"ep": (chip - 1) * 2 + core})
+        greet(same_core(chip - 1))
 
     @pl.when(chip < chips - 1)
     def _():
-        greet({"ep": (chip + 1) * 2 + core})
+        greet(same_core(chip + 1))
 
     def remote(source, target, send, recv, device):
         return pltpu.make_async_remote_copy(
@@ -180,7 +186,7 @@
         )
 
     def ways(way):
-        return ({"ep": (chip - 1) * 2 + core}, {"ep": (chip + 1) * 2 + core}, partner)[way]
+        return (same_core(chip - 1), same_core(chip + 1), partner)[way]
 
     def tokens_copy(origin, way):
         slot = held.at[origin * 2 + core]
@@ -220,21 +226,30 @@
             part_out.at[k], part_in.at[k], part_send.at[0], part_recv.at[place], across
         )
 
-    def shared_part_copy(piece):
+    def shared_part_copy(piece, which):
         return remote(
-            part_out.at[shared_at, piece],
-            part_in.at[shared_at, piece],
+            part_out.at[shared_at, which, :, spans[piece]],
+            part_in.at[shared_at, which, :, spans[piece]],
             part_send.at[0],
             part_recv.at[3 + piece],
             across,
         )
 
+    def shared_part_arrival(piece):
+        return remote(
+            part_out.at[shared_at, :, :, spans[piece]],
+            part_in.at[shared_at, :, :, spans[piece]],
+            part_send.at[0],
+            part_recv.at[3 + piece],
+            across,
+        )
+
     def hidden_copy(k, side):
         slot = hidden.at[k, side]
         return remote(slot, slot, hidden_send.at[0], hidden_recv.at[lax.rem(k, 4)], across)
 
     def shared_copy(piece, side):
-        slot = hidden.at[shared_at, side, :, piece * quarter : (piece + 1) * quarter]
+        slot = hidden.at[shared_at, side, :, spans[piece]]
         return remote(slot, slot, hidden_send.at[0], hidden_recv.at[4 + piece], across)
 
     def part_of(piece):
@@ -266,7 +281,7 @@
             far_in.at[place, :, part_of(piece)],
             far_send.at[0],
             far_recv.at[place, piece],
-            {"ep": target * 2 + core},
+            same_core(target),
         )
 
     def far_arrival(place, piece):
@@ -275,7 +290,7 @@
             far_in.at[place, :, part_of(piece)],
             far_send.at[0],
             far_recv.at[place, piece],
-            {"ep": beside * 2 + core},
+            same_core(beside),
         )
 
     def row_squares(values):
@@ -296,7 +311,27 @@
         return jnp.concatenate([column] * (lanes // 128), axis=1)
 
     loads["tokens"].wait()
-    square_out[0] = pack(row_squares(held[ep].astype(jnp.float32)))
+    def scaled(block):
+        source[...] = (held[block].astype(jnp.float32) * norm_gain_ref[...]).astype(jnp.bfloat16)
+
+    def product_of(matrix, columns):
+        return jnp.dot(
+            source[...], matrix[columns], preferred_element_type=jnp.float32
+        ).astype(jnp.bfloat16)
+
+    def first_gate():
+        loads["gate_away"].wait()
+        part_out[0, 0] = product_of(gate.at[0], (slice(None), away))
+
+    square_out[0] = pack(row_squares(held[me].astype(jnp.float32)))
+    loads["norm_gain"].wait()
+    ahead = chip == 0
+
+    @pl.when(ahead)
+    def _():
+        scaled(me)
+        first_gate()
+
     pl.semaphore_wait(barrier, jnp.where((chip == 0) | (chip == chips - 1), 3, 4))
 
     def send_outward(copy):
@@ -312,7 +347,6 @@
 
     send_outward(tokens_copy)
     square_copy(0).start()
-    loads["norm_gain"].wait()
 
     def share_info():
         loads["table"].wait()
@@ -321,10 +355,10 @@
         for choice in range(routes_ref.shape[0]):
             match = expert_ids == routes_ref[choice : choice + 1, :]
             table = table + jnp.where(match, weights_ref[choice : choice + 1, :], 0.0)
-        info[ep, :experts] = table
+        info[me, :experts] = table
         square_copy(0).wait_recv()
         square = square_out[0] + square_in[0]
-        info[ep, experts:] = lax.rsqrt(square / (2 * width) + epsilon)
+        info[me, experts:] = lax.rsqrt(square / (2 * width) + epsilon)
         send_outward(info_copy)
 
     def take(origin):
@@ -400,14 +434,6 @@
         origin, lane = locate(k)
         return origin * 2 + lane
 
-    def scaled(block):
-        source[...] = (held[block].astype(jnp.float32) * norm_gain_ref[...]).astype(jnp.bfloat16)
-
-    def product_of(matrix, columns):
-        return jnp.dot(
-            source[...], matrix[columns], preferred_element_type=jnp.float32
-        ).astype(jnp.bfloat16)
-
     def first_stage(k):
         origin, lane = locate(k)
         pl.when((k == 2) & (core == 0) & outer)(functools.partial(relay, 2))
@@ -417,9 +443,13 @@
         def _():
             pair_gather_arrival(origin).wait_recv()
 
-        scaled(block_of(k))
-        pl.when(k == 0)(loads["gate_away"].wait)
-        part_out[k, 0] = product_of(gate.at[0], (slice(None), away))
+        pl.when((k == 0) & jnp.logical_not(ahead))(loads["gate_away"].wait)
+
+        @pl.when((k != 0) | jnp.logical_not(ahead))
+        def _():
+            scaled(block_of(k))
+            part_out[k, 0] = product_of(gate.at[0], (slice(None), away))
+
         part_copy(k, 0).start()
 
     def finish_first_stage(k):
@@ -431,35 +461,37 @@
             part_own[k, which] = product_of(matrix.at[0], (slice(None), near))
 
     def piece_of(side, piece):
-        return pl.ds(pl.multiple_of(side * half + piece * quarter, quarter), quarter)
+        start = pl.multiple_of(side * half + cuts[piece], half // 4)
+        return pl.ds(start, cuts[piece + 1] - cuts[piece])
 
     def shared_first(piece):
         if piece == 0:
             loads["shared_in"].wait()
         else:
-            scaled(ep)
+            scaled(me)
         for side, target in ((1 - tp, part_out), (tp, part_own)):
             columns = (slice(None), piece_of(side, piece))
             for which, matrix in enumerate((gate, up)):
-                place = slice(which * quarter, (which + 1) * quarter)
-                target[shared_at, piece, :, place] = product_of(matrix.at[1], columns)
-            if target is part_out:
-                shared_part_copy(piece).start()
+                target[shared_at, which, :, spans[piece]] = product_of(matrix.at[1], columns)
+                if target is part_out:
+                    shared_part_copy(piece, which).start()
 
     def shared_second(piece):
-        scale = across_lanes(unpack(info[ep, experts : experts + 1]), half)
-        shared_part_copy(piece).wait_recv()
-        total = part_own[shared_at, piece].astype(jnp.float32)
-        total = (total + part_in[shared_at, piece].astype(jnp.float32)) * scale
-        product_out = jax.nn.silu(total[:, :quarter]) * total[:, quarter:]
-        place = slice(piece * quarter, (piece + 1) * quarter)
-        hidden[shared_at, tp, :, place] = product_out.astype(jnp.bfloat16)
+        scale = unpack(info[me, experts : experts + 1])
+        scale = across_lanes(scale, cuts[piece + 1] - cuts[piece])
+        shared_part_arrival(piece).wait_recv()
+
+        def total(which):
+            own = part_own[shared_at, which, :, spans[piece]].astype(jnp.float32)
+            return (own + part_in[shared_at, which, :, spans[piece]].astype(jnp.float32)) * scale
+
+        product_out = jax.nn.silu(total(0)) * total(1)
+        hidden[shared_at, tp, :, spans[piece]] = product_out.astype(jnp.bfloat16)
         shared_copy(piece, tp).start()
 
     def shared_product(piece, side, columns):
-        place = slice(piece * quarter, (piece + 1) * quarter)
         return jnp.dot(
-            hidden[shared_at, side, :, place],
+            hidden[shared_at, side, :, spans[piece]],
             down[1, piece_of(side, piece), columns],
             preferred_element_type=jnp.float32,
         )
@@ -581,7 +613,6 @@
         def _():
             pl.when(core == 0)(functools.partial(relay, 1))
             second_stage(0)
-            pl.when((core == 1) & outer)(functools.partial(toward_inner, chip))
 
         @pl.when(i < count)
         def _():
@@ -601,6 +632,7 @@
         def _():
             share_info()
             shared_first(0)
+            pl.when((core == 1) & outer)(functools.partial(toward_inner, chip))
 
         @pl.when(i == 1)
         def _():
@@ -642,19 +674,24 @@
 
     lax.fori_loop(0, count + 2, body, 0)
 
+    def shared_other(columns):
+        mixture[:, columns] += shared_product(1, 1 - tp, columns)
+
+    shared_copy(1, 1 - tp).wait_recv()
+    tiles(shared_other, 0, 2)
+    tiles(shared_other, 2, 4)
+    squares = jnp.zeros((rows, 128), jnp.float32)
     for piece in range(2):
         pair_copy(chip, piece).wait_recv()
         far_arrival(FAR + 1, piece).wait_recv()
         far_arrival(NEAR, piece).wait_recv()
-    shared_copy(1, 1 - tp).wait_recv()
-    squares = jnp.zeros((rows, 128), jnp.float32)
-    for start in range(0, width, tile):
-        columns = slice(start, start + tile)
-        mixed = mixture[:, columns] + shared_product(1, 1 - tp, columns)
-        for arrived in (pair_in.at[chip], far_in.at[FAR + 1], far_in.at[NEAR]):
-            mixed = mixed + arrived[:, columns].astype(jnp.float32)
-        mixture[:, columns] = mixed
-        squares = squares + row_squares(mixed)
+        for start in range(piece * width // 2, (piece + 1) * width // 2, tile):
+            columns = slice(start, start + tile)
+            mixed = mixture[:, columns]
+            for arrived in (pair_in.at[chip], far_in.at[FAR + 1], far_in.at[NEAR]):
+                mixed = mixed + arrived[:, columns].astype(jnp.float32)
+            mixture[:, columns] = mixed
+            squares = squares + row_squares(mixed)
     square_out[1] = pack(squares)
     square_copy(1).start()
     loads["out_gain"].wait()

time: 86.6 us -> 87 us (level); the launches traced: 86.5 us -> 85.3 us
  Pallas kernels: 85.7 us -> 84.5 us
    pallas_call x1, Pallas kernels: 85.7 us -> 84.5 us  [fused(): pl.pallas_call(functools.partial(fused_kernel, chips), out_shape=pltpu.VM...]
where the time goes in v7:
time: 87 us; the launch traced here: 85.3 us
  Pallas kernels  84.5 us (97%)
    pallas_call x1, Pallas kernels, fused(): pl.pallas_call(functools.partial(fused_kernel, chips), out_shape=pltpu.VM...  84.5 us

profile of v7, /device:TPU:1, one launch (start us, length us, event | category | flops | bytes accessed | tf_op | source)
XLA Modules:
  0.0 85.3 jit_solution(8569196164135619249)
XLA Ops:
  0.0 84.5 %shard_map.109 = bf16[128,2048]{1,0:T(8,128)(2,1)S(1)} custom-call(bf16[128,2048]{1,0:T(8,128)(2,1)} %tokens_hbm.1, s32[4,128]{1,0:T(4,128)} %bitcast.6, f32[4,128]{1,0:T(4,128)} %bitcast.7, f32[1,4096]{1,0:T(1,128)} %bitcast.4, bf16[1,2048,1024]{2,1,0:T(8,128)(2,1)} %gate_hbm.1, bf16[1,2048,1024]{2,1,0:T(8,128)(2,1)} %up_hbm.1, ...), custom_call_target="tpu_custom_call" | custom-call | tf_op jit(solution)/shard_map/pallas_call | solution.py:750
  84.5 0.8 copy.13
